TPU v7x, 256 devices: a whole 4x4x8 slice. The times are simulated.
256 devices in a mesh: sp: 32 (over z, y), tp: 8 (over x, core).
Axes of the slice: x: 4, y: 4, z: 8, core: 2. Of those that a mesh axis runs over, the one named last changes fastest.
Arguments:
- resid: bfloat16 [16384, 2048], P('sp', 'tp'), may hold values from -41 to 41
- queries: bfloat16 [16384, 1024], P('sp', 'tp'), may hold values from -6 to 6
- keys: bfloat16 [16384, 1024], P('sp', 'tp'), may hold values from -6 to 6
- values: bfloat16 [16384, 1024], P('sp', 'tp'), may hold values from -6 to 6
- mix_lambda: float32 [8], P('tp'), may hold values from 0.3 to 0.8
- head_gain: float32 [128], replicated, may hold values from 0.1 to 1.9
- out_weight: bfloat16 [1024, 2048], P(None, 'tp'), may hold values from -0.1875 to 0.1875
- norm_gain: float32 [2048], P('tp'), may hold values from 0.1 to 1.9
- gate_weight: bfloat16 [2048, 5632], P('sp', 'tp'), may hold values from -0.125 to 0.125
- up_weight: bfloat16 [2048, 5632], P('sp', 'tp'), may hold values from -0.125 to 0.125
- conv_weight: float32 [3, 5632], P(None, 'tp'), may hold values from -3.5 to 3.5
- conv_bias: float32 [5632], P('tp'), may hold values from -3 to 3
- down_weight: bfloat16 [5632, 2048], P('tp', 'sp'), may hold values from -0.078125 to 0.078125
Outputs:
- layer_out: bfloat16 [16384, 2048], P('sp', 'tp')
All inputs are finite; a program needn't handle non-finite values.
Results may differ from a plain program's by a relative error of at most 0.009.
Values may be sent and summed in bfloat16 or wider, within the bound.
A program may use at most 128 MiB of HBM per device.

v0:
```python
import math

import jax
import jax.numpy as jnp
from jax import lax
from jax.sharding import Mesh
from jax.sharding import PartitionSpec as P

D = 2048
HD = 64
VD = 128
SP = ("sp_0", "sp_1")


def whole_of(array, axes, dim):
    if not axes:
        return array
    nearer = lax.all_gather(array, axes[-1], axis=dim, tiled=True)
    return whole_of(nearer, axes[:-1], dim)


def sent_together(arrays, axis, dim, along):
    both = jnp.concatenate(arrays, axis=along)
    out, at, gathered = (lax.all_gather(both, axis, axis=dim, tiled=True), 0, [])
    for a in arrays:
        gathered.append(lax.slice_in_dim(out, at, at + a.shape[along], axis=along))
        at += a.shape[along]
    return tuple(gathered)


def sent_to_all(array, axis):
    copies = jnp.broadcast_to(array, (lax.axis_size(axis), *array.shape))
    return lax.all_to_all(copies, axis, split_axis=0, concat_axis=0, tiled=True)


def joined_along(pieces, dim):
    lengths = list(pieces.shape[1:])
    lengths[dim] *= pieces.shape[0]
    return jnp.moveaxis(pieces, 0, dim).reshape(lengths)


def collect(array, axis, dim):
    pieces = sent_to_all(array, axis)
    return joined_along(pieces, dim)


def of_everyone(array, axis):
    everything = sent_to_all(array, axis)
    return jnp.sum(everything, axis=0)


def with_halo(cells, sides, width):
    for axis, dim in sides:
        count = lax.axis_size(axis)
        ends = count - 1
        head = lax.slice_in_dim(cells, 0, width, axis=dim)
        tail = lax.slice_in_dim(cells, cells.shape[dim] - width, cells.shape[dim], axis=dim)
        cells = jnp.concatenate(
            [
                lax.ppermute(tail, axis, [(i, (i + 1) % count) for i in range(ends)]),
                cells,
                lax.ppermute(head, axis, [((i + 1) % count, i) for i in range(ends)]),
            ],
            axis=dim,
        )
    return cells


def split_up(array, dim, devices):
    before, after = (array.shape[:dim], array.shape[dim + 1 :])
    return jnp.moveaxis(array.reshape(*before, devices, -1, *after), dim, 0)


def sent_and_summed(array, axis, dim):
    devices = lax.axis_size(axis)
    pieces = lax.all_to_all(split_up(array, dim, devices), axis, 0, 0, tiled=True)
    return jnp.sum(pieces.astype(jnp.float32), axis=0)


def on_device(
    resid,
    queries,
    keys,
    values,
    mix_lambda,
    head_gain,
    out_weight,
    norm_gain,
    gate_weight,
    up_weight,
    conv_weight,
    conv_bias,
    down_weight,
):
    length = queries.shape[0]
    heads = mix_lambda.shape[0]
    scale = HD ** (-0.5)
    gate_whole, up_whole = (whole_of(gate_weight, SP, 0), whole_of(up_weight, SP, 0))
    down_whole = whole_of(down_weight, SP, 1)
    query_heads = queries.reshape(length, heads, 2, HD)
    initial = (
        jnp.full((heads, 2, length), -1e30, jnp.float32),
        jnp.zeros((heads, 2, length), jnp.float32),
        jnp.zeros((heads, 2, length, VD), jnp.float32),
    )
    key_rows, value_rows = sent_together((keys, values), SP, 0, 1)
    count = key_rows.shape[0]
    block = math.gcd(count, 2048)
    key_blocks = key_rows.reshape(count // block, block, heads, 2, HD)
    value_blocks = value_rows.reshape(count // block, block, heads, VD)

    def advance(state, blocks):
        running, totals, weighted = state
        key_block, value_block = blocks
        scores = (
            jnp.einsum(
                "qhmd,khmd->hmqk", query_heads, key_block, preferred_element_type=jnp.float32
            )
            * scale
        )
        highest = jnp.maximum(running, jnp.max(scores, axis=-1))
        factor = jnp.exp(running - highest)
        shifted = jnp.exp(scores - highest[..., None])
        totals = totals * factor + jnp.sum(shifted, axis=-1)
        weighted = weighted * factor[..., None] + jnp.einsum(
            "hmqk,khe->hmqe",
            shifted.astype(jnp.bfloat16),
            value_block,
            preferred_element_type=jnp.float32,
        )
        return ((highest, totals, weighted), None)

    result, unused = lax.scan(advance, initial, (key_blocks, value_blocks))
    running, totals, weighted = result
    mapped = weighted / totals[..., None]
    mixed = mapped[:, 0] - mix_lambda[:, None, None] * mapped[:, 1]
    spread = jnp.mean(mixed * mixed, axis=-1, keepdims=True)
    normed = mixed * lax.rsqrt(spread + 1e-06) * head_gain * 0.8
    heads_out = jnp.transpose(normed, (1, 0, 2)).reshape(length, heads * VD).astype(jnp.bfloat16)
    projected = jnp.dot(collect(heads_out, "tp", 1), out_weight, preferred_element_type=jnp.float32)
    after_mixer = resid.astype(jnp.float32) + projected
    squares = of_everyone(jnp.sum(after_mixer * after_mixer, axis=1), "tp")
    normed_rows = (after_mixer * lax.rsqrt(squares / D + 1e-06)[:, None] * norm_gain).astype(
        jnp.bfloat16
    )
    full_rows = collect(normed_rows, "tp", 1)
    gate_sum = jnp.dot(full_rows, gate_whole, preferred_element_type=jnp.float32)
    upward = jnp.dot(full_rows, up_whole, preferred_element_type=jnp.float32)
    gated = gate_sum.astype(jnp.bfloat16)
    padded = with_halo(gated, ((SP, 0),), 1).astype(jnp.float32)
    conv = (
        padded[:-2] * conv_weight[0]
        + padded[1:-1] * conv_weight[1]
        + padded[2:] * conv_weight[2]
        + conv_bias
    )
    hidden = (jax.nn.silu(conv) * upward).astype(jnp.bfloat16)
    partial_terms = jnp.dot(hidden, down_whole, preferred_element_type=jnp.float32)
    mixer_out = sent_and_summed(partial_terms.astype(jnp.bfloat16), "tp", 1)
    return (after_mixer + mixer_out).astype(jnp.bfloat16)


def solution(mesh):
    torus = Mesh(mesh.devices.reshape(8, 4, mesh.shape["tp"]), ("sp_0", "sp_1", "tp"))
    return jax.shard_map(
        on_device,
        mesh=torus,
        in_specs=(
            P(SP, "tp"),
            P(SP, "tp"),
            P(SP, "tp"),
            P(SP, "tp"),
            P("tp"),
            P(),
            P(None, "tp"),
            P("tp"),
            P(SP, "tp"),
            P(SP, "tp"),
            P(None, "tp"),
            P("tp"),
            P("tp", SP),
        ),
        out_specs=P(SP, "tp"),
        check_vma=False,
    )
```

profile of v0, /device:TPU:1, one launch (start us, length us, event | category | flops | bytes accessed | tf_op | source)
XLA Modules:
  0.0 383.1 jit_solution(15060933424168356836)
XLA Ops:
  6.5 1.8 pad_maximum_fusion
  8.4 13.0 %all_gather.22 = bf16[256,704]{1,0:T(8,128)(2,1)} all-gather(bf16[64,704]{1,0:T(8,128)(2,1)} %param.23), channel_id=1, replica_groups=mesh['sp_0'=8,'sp_1'=4,'tp'=8] {'sp_1'}, dimensions={0}, use_global_device_ids=true | all-gather | bytes 450560 | tf_op jit(solution)/shard_map/all_gather | solution.py:18
  21.5 11.4 %all_gather.26 = bf16[704,256]{0,1:T(8,128)(2,1)} all-gather(bf16[704,64]{0,1:T(8,128)(2,1)} %param.27), channel_id=1, replica_groups=mesh['sp_0'=8,'sp_1'=4,'tp'=8] {'sp_1'}, dimensions={1}, use_global_device_ids=true | all-gather | bytes 450560 | tf_op jit(solution)/shard_map/all_gather | solution.py:18
  33.0 12.0 %all_gather.24 = bf16[256,704]{1,0:T(8,128)(2,1)} all-gather(bf16[64,704]{1,0:T(8,128)(2,1)} %param.24), channel_id=1, replica_groups=mesh['sp_0'=8,'sp_1'=4,'tp'=8] {'sp_1'}, dimensions={0}, use_global_device_ids=true | all-gather | bytes 450560 | tf_op jit(solution)/shard_map/all_gather | solution.py:18
  45.8 65.2 %all-gather.5.cloned.1.call-done = bf16[16384,256]{1,0:T(8,128)(2,1)} async-done(((bf16[512,256]{1,0:T(8,128)(2,1)}), bf16[16384,256]{1,0:T(8,128)(2,1)}) %all-gather.5.cloned.1.call-update) | async-done | bytes 8388624 | tf_op jit(solution)/shard_map/all_gather | solution.py:24
  111.0 5.7 %fusion.35 = (bf16[16384,128]{1,0:T(8,128)(2,1)}, bf16[16384,128]{1,0:T(8,128)(2,1)}) fusion(bf16[16384,256]{1,0:T(8,128)(2,1)} %all-gather.5.cloned.1.call-done), kind=kLoop, calls=%fused_computation.61 | loop fusion | bytes 16777216 | tf_op jit(solution)/shard_map/slice | solution.py:26
  116.7 14.7 %reshape.145 = bf16[8,2048,1,2,64]{4,3,1,0,2:T(2,128)(2,1)} reshape(bf16[16384,128]{1,0:T(8,128)(2,1)} %get-tuple-element.119) | data formatting | bytes 8388608 | tf_op jit(solution)/shard_map/reshape | solution.py:109
  131.4 20.2 %copy.50 = bf16[8,2048,1,2,64]{1,4,3,2,0:T(8,128)(2,1)} copy(bf16[8,2048,1,2,64]{4,3,1,0,2:T(2,128)(2,1)} %reshape.145) | data formatting | bytes 8388608
  151.7 104.1 %while.15 = (s32[]{:T(128)}, f32[1,2,512]{2,1,0:T(2,128)S(1)}, f32[1,2,512]{2,1,0:T(2,128)S(1)}, f32[1,2,512,128]{3,2,1,0:T(8,128)S(1)}, bf16[8,2048,1,2,64]{1,4...) while((s32[]{:T(128)}, f32[1,2,512]{2,1,0:T(2,128)S(1)}, ...), condition=%wide.region_3.4_spmd.clone, body=%wide.region_0.3_spmd.clone.sunk | while | flops 822482944 | bytes 61015168 | solution.py:133
  151.7 5.6 %bitcast_reduce_fusion.2 = (f32[2,512]{1,0:T(2,128)S(1)}, f32[2,2048,512]{2,1,0:T(8,128)}) fusion(bf16[512,1,2,64]{0,3,2,1:T(8,128)(2,1)S(1)} %get-tuple-element.198, bf16[8,2048,1,2,64]{1,4,3,2,0:T(8,128)(2,1)} %get-tuple-element.197, s32[]{:T(128)} %get-tuple-element.184), kind=kOutput, calls=%fused_computation.1.clone.1 | convolution fusion | flops 272628736 | bytes 9048576 | tf_op jit(solution)/shard_map/while/body/eval_jaxpr/qhmd,khmd->hmqk/dot_general | solution.py:116
  157.3 5.3 %fusion.53 = f32[1,2,512,128]{3,2,1,0:T(8,128)S(1)} fusion(f32[2,2048,512]{2,1,0:T(8,128)} %get-tuple-element.173, f32[2,512]{1,0:T(2,128)S(1)} %bitcast.98, f32[1,2,512,128]{3,2,1,0:T(8,128)S(1)} %get-tuple-element.187, bf16[8,2048,1,128]{3,1,2,0:T(8,128)(2,1)} %get-tuple-element.199, s32[]{:T(128)} %get-tuple-element.184, ...), kind=kOutput, calls=%fused_computation.7.clone.1 | convolution fusion | flops 543555584 | bytes 9970177 | tf_op jit(solution)/shard_map/while/body/eval_jaxpr/hmqk,khe->hmqe/dot_general | solution.py:125
  162.5 0.6 copy-done.1
  163.2 1.4 fusion.52
  164.6 5.6 %bitcast_reduce_fusion.2 = (f32[2,512]{1,0:T(2,128)S(1)}, f32[2,2048,512]{2,1,0:T(8,128)}) fusion(bf16[512,1,2,64]{0,3,2,1:T(8,128)(2,1)S(1)} %get-tuple-element.198, bf16[8,2048,1,2,64]{1,4,3,2,0:T(8,128)(2,1)} %get-tuple-element.197, s32[]{:T(128)} %get-tuple-element.184), kind=kOutput, calls=%fused_computation.1.clone.1 | convolution fusion | flops 272628736 | bytes 9048576 | tf_op jit(solution)/shard_map/while/body/eval_jaxpr/qhmd,khmd->hmqk/dot_general | solution.py:116
  170.2 5.3 %fusion.53 = f32[1,2,512,128]{3,2,1,0:T(8,128)S(1)} fusion(f32[2,2048,512]{2,1,0:T(8,128)} %get-tuple-element.173, f32[2,512]{1,0:T(2,128)S(1)} %bitcast.98, f32[1,2,512,128]{3,2,1,0:T(8,128)S(1)} %get-tuple-element.187, bf16[8,2048,1,128]{3,1,2,0:T(8,128)(2,1)} %get-tuple-element.199, s32[]{:T(128)} %get-tuple-element.184, ...), kind=kOutput, calls=%fused_computation.7.clone.1 | convolution fusion | flops 543555584 | bytes 9970177 | tf_op jit(solution)/shard_map/while/body/eval_jaxpr/hmqk,khe->hmqe/dot_general | solution.py:125
  175.5 0.7 copy-done.1
  176.2 1.4 fusion.52
  177.6 5.6 %bitcast_reduce_fusion.2 = (f32[2,512]{1,0:T(2,128)S(1)}, f32[2,2048,512]{2,1,0:T(8,128)}) fusion(bf16[512,1,2,64]{0,3,2,1:T(8,128)(2,1)S(1)} %get-tuple-element.198, bf16[8,2048,1,2,64]{1,4,3,2,0:T(8,128)(2,1)} %get-tuple-element.197, s32[]{:T(128)} %get-tuple-element.184), kind=kOutput, calls=%fused_computation.1.clone.1 | convolution fusion | flops 272628736 | bytes 9048576 | tf_op jit(solution)/shard_map/while/body/eval_jaxpr/qhmd,khmd->hmqk/dot_general | solution.py:116
  183.2 5.3 %fusion.53 = f32[1,2,512,128]{3,2,1,0:T(8,128)S(1)} fusion(f32[2,2048,512]{2,1,0:T(8,128)} %get-tuple-element.173, f32[2,512]{1,0:T(2,128)S(1)} %bitcast.98, f32[1,2,512,128]{3,2,1,0:T(8,128)S(1)} %get-tuple-element.187, bf16[8,2048,1,128]{3,1,2,0:T(8,128)(2,1)} %get-tuple-element.199, s32[]{:T(128)} %get-tuple-element.184, ...), kind=kOutput, calls=%fused_computation.7.clone.1 | convolution fusion | flops 543555584 | bytes 9970177 | tf_op jit(solution)/shard_map/while/body/eval_jaxpr/hmqk,khe->hmqe/dot_general | solution.py:125
  188.6 0.7 copy-done.1
  189.3 1.4 fusion.52
  190.7 5.6 %bitcast_reduce_fusion.2 = (f32[2,512]{1,0:T(2,128)S(1)}, f32[2,2048,512]{2,1,0:T(8,128)}) fusion(bf16[512,1,2,64]{0,3,2,1:T(8,128)(2,1)S(1)} %get-tuple-element.198, bf16[8,2048,1,2,64]{1,4,3,2,0:T(8,128)(2,1)} %get-tuple-element.197, s32[]{:T(128)} %get-tuple-element.184), kind=kOutput, calls=%fused_computation.1.clone.1 | convolution fusion | flops 272628736 | bytes 9048576 | tf_op jit(solution)/shard_map/while/body/eval_jaxpr/qhmd,khmd->hmqk/dot_general | solution.py:116
  196.3 5.3 %fusion.53 = f32[1,2,512,128]{3,2,1,0:T(8,128)S(1)} fusion(f32[2,2048,512]{2,1,0:T(8,128)} %get-tuple-element.173, f32[2,512]{1,0:T(2,128)S(1)} %bitcast.98, f32[1,2,512,128]{3,2,1,0:T(8,128)S(1)} %get-tuple-element.187, bf16[8,2048,1,128]{3,1,2,0:T(8,128)(2,1)} %get-tuple-element.199, s32[]{:T(128)} %get-tuple-element.184, ...), kind=kOutput, calls=%fused_computation.7.clone.1 | convolution fusion | flops 543555584 | bytes 9970177 | tf_op jit(solution)/shard_map/while/body/eval_jaxpr/hmqk,khe->hmqe/dot_general | solution.py:125
  201.6 0.7 copy-done.1
  202.2 1.4 fusion.52
  203.7 5.6 %bitcast_reduce_fusion.2 = (f32[2,512]{1,0:T(2,128)S(1)}, f32[2,2048,512]{2,1,0:T(8,128)}) fusion(bf16[512,1,2,64]{0,3,2,1:T(8,128)(2,1)S(1)} %get-tuple-element.198, bf16[8,2048,1,2,64]{1,4,3,2,0:T(8,128)(2,1)} %get-tuple-element.197, s32[]{:T(128)} %get-tuple-element.184), kind=kOutput, calls=%fused_computation.1.clone.1 | convolution fusion | flops 272628736 | bytes 9048576 | tf_op jit(solution)/shard_map/while/body/eval_jaxpr/qhmd,khmd->hmqk/dot_general | solution.py:116
  209.3 5.3 %fusion.53 = f32[1,2,512,128]{3,2,1,0:T(8,128)S(1)} fusion(f32[2,2048,512]{2,1,0:T(8,128)} %get-tuple-element.173, f32[2,512]{1,0:T(2,128)S(1)} %bitcast.98, f32[1,2,512,128]{3,2,1,0:T(8,128)S(1)} %get-tuple-element.187, bf16[8,2048,1,128]{3,1,2,0:T(8,128)(2,1)} %get-tuple-element.199, s32[]{:T(128)} %get-tuple-element.184, ...), kind=kOutput, calls=%fused_computation.7.clone.1 | convolution fusion | flops 543555584 | bytes 9970177 | tf_op jit(solution)/shard_map/while/body/eval_jaxpr/hmqk,khe->hmqe/dot_general | solution.py:125
  214.5 0.8 copy-done.1
  215.3 1.4 fusion.52
  216.7 5.6 %bitcast_reduce_fusion.2 = (f32[2,512]{1,0:T(2,128)S(1)}, f32[2,2048,512]{2,1,0:T(8,128)}) fusion(bf16[512,1,2,64]{0,3,2,1:T(8,128)(2,1)S(1)} %get-tuple-element.198, bf16[8,2048,1,2,64]{1,4,3,2,0:T(8,128)(2,1)} %get-tuple-element.197, s32[]{:T(128)} %get-tuple-element.184), kind=kOutput, calls=%fused_computation.1.clone.1 | convolution fusion | flops 272628736 | bytes 9048576 | tf_op jit(solution)/shard_map/while/body/eval_jaxpr/qhmd,khmd->hmqk/dot_general | solution.py:116
  222.3 5.3 %fusion.53 = f32[1,2,512,128]{3,2,1,0:T(8,128)S(1)} fusion(f32[2,2048,512]{2,1,0:T(8,128)} %get-tuple-element.173, f32[2,512]{1,0:T(2,128)S(1)} %bitcast.98, f32[1,2,512,128]{3,2,1,0:T(8,128)S(1)} %get-tuple-element.187, bf16[8,2048,1,128]{3,1,2,0:T(8,128)(2,1)} %get-tuple-element.199, s32[]{:T(128)} %get-tuple-element.184, ...), kind=kOutput, calls=%fused_computation.7.clone.1 | convolution fusion | flops 543555584 | bytes 9970177 | tf_op jit(solution)/shard_map/while/body/eval_jaxpr/hmqk,khe->hmqe/dot_general | solution.py:125
  227.7 0.7 copy-done.1
  228.4 1.4 fusion.52
  229.8 5.6 %bitcast_reduce_fusion.2 = (f32[2,512]{1,0:T(2,128)S(1)}, f32[2,2048,512]{2,1,0:T(8,128)}) fusion(bf16[512,1,2,64]{0,3,2,1:T(8,128)(2,1)S(1)} %get-tuple-element.198, bf16[8,2048,1,2,64]{1,4,3,2,0:T(8,128)(2,1)} %get-tuple-element.197, s32[]{:T(128)} %get-tuple-element.184), kind=kOutput, calls=%fused_computation.1.clone.1 | convolution fusion | flops 272628736 | bytes 9048576 | tf_op jit(solution)/shard_map/while/body/eval_jaxpr/qhmd,khmd->hmqk/dot_general | solution.py:116
  235.4 5.3 %fusion.53 = f32[1,2,512,128]{3,2,1,0:T(8,128)S(1)} fusion(f32[2,2048,512]{2,1,0:T(8,128)} %get-tuple-element.173, f32[2,512]{1,0:T(2,128)S(1)} %bitcast.98, f32[1,2,512,128]{3,2,1,0:T(8,128)S(1)} %get-tuple-element.187, bf16[8,2048,1,128]{3,1,2,0:T(8,128)(2,1)} %get-tuple-element.199, s32[]{:T(128)} %get-tuple-element.184, ...), kind=kOutput, calls=%fused_computation.7.clone.1 | convolution fusion | flops 543555584 | bytes 9970177 | tf_op jit(solution)/shard_map/while/body/eval_jaxpr/hmqk,khe->hmqe/dot_general | solution.py:125
  240.7 0.7 copy-done.1
  241.5 1.4 fusion.52
  242.9 5.6 %bitcast_reduce_fusion.2 = (f32[2,512]{1,0:T(2,128)S(1)}, f32[2,2048,512]{2,1,0:T(8,128)}) fusion(bf16[512,1,2,64]{0,3,2,1:T(8,128)(2,1)S(1)} %get-tuple-element.198, bf16[8,2048,1,2,64]{1,4,3,2,0:T(8,128)(2,1)} %get-tuple-element.197, s32[]{:T(128)} %get-tuple-element.184), kind=kOutput, calls=%fused_computation.1.clone.1 | convolution fusion | flops 272628736 | bytes 9048576 | tf_op jit(solution)/shard_map/while/body/eval_jaxpr/qhmd,khmd->hmqk/dot_general | solution.py:116
  248.5 5.3 %fusion.53 = f32[1,2,512,128]{3,2,1,0:T(8,128)S(1)} fusion(f32[2,2048,512]{2,1,0:T(8,128)} %get-tuple-element.173, f32[2,512]{1,0:T(2,128)S(1)} %bitcast.98, f32[1,2,512,128]{3,2,1,0:T(8,128)S(1)} %get-tuple-element.187, bf16[8,2048,1,128]{3,1,2,0:T(8,128)(2,1)} %get-tuple-element.199, s32[]{:T(128)} %get-tuple-element.184, ...), kind=kOutput, calls=%fused_computation.7.clone.1 | convolution fusion | flops 543555584 | bytes 9970177 | tf_op jit(solution)/shard_map/while/body/eval_jaxpr/hmqk,khe->hmqe/dot_general | solution.py:125
  253.7 0.6 copy-done.1
  254.4 1.4 fusion.52
  255.8 0.2 broadcast_divide_fusion
  256.0 0.1 multiply_reduce_fusion.1
  256.5 1.1 broadcast_in_dim.30
  257.5 5.7 %all-to-all-start = ((bf16[8,512,128]{1,2,0:T(8,128)(2,1)}), bf16[8,512,128]{1,2,0:T(8,128)(2,1)S(1)}, u32[]{:S(2)}, u32[]{:S(2)}) async-start(bf16[8,512,128]{1,2,0:T(8,128)(2,1)} %broadcast_in_dim.30), calls=%async_computation | async-start | bytes 2097152 | tf_op jit(solution)/shard_map/all_to_all | solution.py:33
  263.2 0.1 copy.47
  263.3 14.8 %all-to-all-done = bf16[8,512,128]{1,2,0:T(8,128)(2,1)S(1)} async-done(((bf16[8,512,128]{1,2,0:T(8,128)(2,1)}), bf16[8,512,128]{1,2,0:T(8,128)(2,1)S(1)}, u32[]{:S(2)}, u32[]{:S(2)}) %all-to-all-start) | async-done | bytes 1048608 | tf_op jit(solution)/shard_map/all_to_all | solution.py:33
  278.2 0.5 multiply_reduce_fusion
  278.7 8.0 %all_to_all.21 = f32[8,1,512]{2,1,0:T(1,128)S(1)} all-to-all(f32[8,1,512]{2,1,0:T(1,128)S(1)} %broadcast_in_dim.31), channel_id=1, replica_groups=mesh['sp_0'=8,'sp_1'=4,'tp'=8] {'tp'}, dimensions={0} | all-to-all | bytes 32768 | tf_op jit(solution)/shard_map/all_to_all | solution.py:33
  286.8 1.5 broadcast_in_dim.32
  288.4 4.2 %all-to-all-start.2 = ((bf16[8,512,256]{1,2,0:T(8,128)(2,1)}), bf16[8,512,256]{1,2,0:T(8,128)(2,1)S(1)}, u32[]{:S(2)}, u32[]{:S(2)}) async-start(bf16[8,512,256]{1,2,0:T(8,128)(2,1)} %broadcast_in_dim.32), calls=%async_computation.2 | async-start | bytes 4194304 | tf_op jit(solution)/shard_map/all_to_all | solution.py:33
  292.6 26.2 %all-to-all-done.2 = bf16[8,512,256]{1,2,0:T(8,128)(2,1)S(1)} async-done(((bf16[8,512,256]{1,2,0:T(8,128)(2,1)}), bf16[8,512,256]{1,2,0:T(8,128)(2,1)S(1)}, u32[]{:S(2)}, u32[]{:S(2)}) %all-to-all-start.2) | async-done | bytes 2097184 | tf_op jit(solution)/shard_map/all_to_all | solution.py:33
  318.8 3.6 convolution_convert_fusion.1
  322.5 1.9 collective-permute-start
  324.4 1.5 collective-permute-start.1
  326.0 1.4 collective-permute-done
  327.3 3.8 %collective-permute-done.1 = bf16[1,704]{0,1:T(8,128)(2,1)S(1)} collective-permute-done((bf16[1,704]{0,1:T(8,128)(2,1)S(1)}, bf16[1,704]{0,1:T(8,128)(2,1)S(1)}, u32[]{:S(2)}, u32[]{:S(2)}) %collective-permute-start.1) | collective-permute-done | bytes 1440 | tf_op jit(solution)/shard_map/ppermute | solution.py:62
  331.2 1.6 maximum_convert_fusion
  332.8 9.8 %convolution_convert_fusion = bf16[512,2048]{1,0:T(8,128)(2,1)} fusion(bf16[704,2048]{0,1:T(8,128)(2,1)} %all-gather.11.cloned.1.call-done, bf16[512,2048]{0,1:T(8,128)(2,1)S(1)} %bitcast.101, bf16[2048,704]{1,0:T(8,128)(2,1)} %all-gather.9.cloned.1.call-done, f32[514,704]{0,1:T(8,128)} %maximum_convert_fusion, f32[704]{0:T(1024)S(1)} %copy-done.7, ...), kind=kOutput, calls=%fused_computation.25 | convolution fusion | flops 2958163968 | bytes 14822400 | tf_op jit(solution)/shard_map/dot_general | solution.py:158
  342.7 1.7 copy.64
  344.4 30.7 %all_to_all.22 = bf16[8,512,256]{2,1,0:T(8,128)(2,1)S(1)} all-to-all(bf16[8,512,256]{2,1,0:T(8,128)(2,1)S(1)} %bitcast.96), channel_id=1, replica_groups=mesh['sp_0'=8,'sp_1'=4,'tp'=8] {'tp'}, dimensions={0} | all-to-all | bytes 4194304 | tf_op jit(solution)/shard_map/all_to_all | solution.py:76
  375.1 0.3 convert_reduce_fusion
  375.4 0.2 copy.55
  375.7 0.8 copy.56
  (71 shorter events, 1.3 us)
Async XLA Ops:
  6.5 271.6 %copy-start = (bf16[1024,256]{1,0:T(8,128)(2,1)S(1)}, bf16[1024,256]{1,0:T(8,128)(2,1)}, u32[]{:S(2)}) copy-start(bf16[1024,256]{1,0:T(8,128)(2,1)} %param.21) | copy-start | bytes 1572868
  6.5 38.5 %copy-start.3 = (bf16[512,128]{1,0:T(8,128)(2,1)S(1)}, bf16[512,128]{1,0:T(8,128)(2,1)}, u32[]{:S(2)}) copy-start(bf16[512,128]{1,0:T(8,128)(2,1)} %param.16) | copy-start | bytes 393220
  6.5 104.5 %all-gather.5.cloned.1.call-start = ((), (), s32[]{:S(2)}) async-start(), calls=%async_computation.4 | async-start | bytes 8650752 | tf_op jit(solution)/shard_map/all_gather | solution.py:24
  8.3 284.2 %all-gather.7.cloned.1.call-start = ((), (), s32[]{:S(2)}) async-start(), calls=%async_computation.5 | async-start | bytes 3538944 | tf_op jit(solution)/shard_map/all_gather | solution.py:18
  21.4 311.4 %all-gather.11.cloned.1.call-start = ((), (), s32[]{:S(2)}) async-start(), calls=%async_computation.7 | async-start | bytes 3538944 | tf_op jit(solution)/shard_map/all_gather | solution.py:18
  32.9 299.9 %all-gather.9.cloned.1.call-start = ((), (), s32[]{:S(2)}) async-start(), calls=%async_computation.6 | async-start | bytes 3538944 | tf_op jit(solution)/shard_map/all_gather | solution.py:18
  151.7 104.5 %copy-start.6 = (f32[128]{0:T(128)S(1)}, f32[128]{0:T(128)}, u32[]{:S(2)}) copy-start(f32[128]{0:T(128)} %param.20) | copy-start | bytes 1540
  157.3 5.9 %copy-start.1 = (f32[2,2048,512]{2,1,0:T(8,128)S(1)}, f32[2,2048,512]{2,1,0:T(8,128)}, u32[]{:S(2)}) copy-start(f32[2,2048,512]{2,1,0:T(8,128)} %get-tuple-element.173) | copy-start | bytes 25165828 | tf_op jit(solution)/shard_map/while
  170.2 6.0 %copy-start.1 = (f32[2,2048,512]{2,1,0:T(8,128)S(1)}, f32[2,2048,512]{2,1,0:T(8,128)}, u32[]{:S(2)}) copy-start(f32[2,2048,512]{2,1,0:T(8,128)} %get-tuple-element.173) | copy-start | bytes 25165828 | tf_op jit(solution)/shard_map/while
  183.2 6.1 %copy-start.1 = (f32[2,2048,512]{2,1,0:T(8,128)S(1)}, f32[2,2048,512]{2,1,0:T(8,128)}, u32[]{:S(2)}) copy-start(f32[2,2048,512]{2,1,0:T(8,128)} %get-tuple-element.173) | copy-start | bytes 25165828 | tf_op jit(solution)/shard_map/while
  196.3 5.9 %copy-start.1 = (f32[2,2048,512]{2,1,0:T(8,128)S(1)}, f32[2,2048,512]{2,1,0:T(8,128)}, u32[]{:S(2)}) copy-start(f32[2,2048,512]{2,1,0:T(8,128)} %get-tuple-element.173) | copy-start | bytes 25165828 | tf_op jit(solution)/shard_map/while
  209.2 6.1 %copy-start.1 = (f32[2,2048,512]{2,1,0:T(8,128)S(1)}, f32[2,2048,512]{2,1,0:T(8,128)}, u32[]{:S(2)}) copy-start(f32[2,2048,512]{2,1,0:T(8,128)} %get-tuple-element.173) | copy-start | bytes 25165828 | tf_op jit(solution)/shard_map/while
  222.3 6.1 %copy-start.1 = (f32[2,2048,512]{2,1,0:T(8,128)S(1)}, f32[2,2048,512]{2,1,0:T(8,128)}, u32[]{:S(2)}) copy-start(f32[2,2048,512]{2,1,0:T(8,128)} %get-tuple-element.173) | copy-start | bytes 25165828 | tf_op jit(solution)/shard_map/while
  235.4 6.1 %copy-start.1 = (f32[2,2048,512]{2,1,0:T(8,128)S(1)}, f32[2,2048,512]{2,1,0:T(8,128)}, u32[]{:S(2)}) copy-start(f32[2,2048,512]{2,1,0:T(8,128)} %get-tuple-element.173) | copy-start | bytes 25165828 | tf_op jit(solution)/shard_map/while
  248.5 5.9 %copy-start.1 = (f32[2,2048,512]{2,1,0:T(8,128)S(1)}, f32[2,2048,512]{2,1,0:T(8,128)}, u32[]{:S(2)}) copy-start(f32[2,2048,512]{2,1,0:T(8,128)} %get-tuple-element.173) | copy-start | bytes 25165828 | tf_op jit(solution)/shard_map/while
  255.8 7.4 %copy-start.2 = (bf16[512,256]{1,0:T(8,128)(2,1)S(1)}, bf16[512,256]{1,0:T(8,128)(2,1)}, u32[]{:S(2)}) copy-start(bf16[512,256]{1,0:T(8,128)(2,1)} %param.15) | copy-start | bytes 786436
  256.5 30.2 %copy-start.5 = (f32[256]{0:T(256)S(1)}, f32[256]{0:T(256)}, u32[]{:S(2)}) copy-start(f32[256]{0:T(256)} %param.22) | copy-start | bytes 3076
  257.5 20.6 %all-to-all-start = ((bf16[8,512,128]{1,2,0:T(8,128)(2,1)}), bf16[8,512,128]{1,2,0:T(8,128)(2,1)S(1)}, u32[]{:S(2)}, u32[]{:S(2)}) async-start(bf16[8,512,128]{1,2,0:T(8,128)(2,1)} %broadcast_in_dim.30), calls=%async_computation | async-start | bytes 2097152 | tf_op jit(solution)/shard_map/all_to_all | solution.py:33
  288.4 30.4 %all-to-all-start.2 = ((bf16[8,512,256]{1,2,0:T(8,128)(2,1)}), bf16[8,512,256]{1,2,0:T(8,128)(2,1)S(1)}, u32[]{:S(2)}, u32[]{:S(2)}) async-start(bf16[8,512,256]{1,2,0:T(8,128)(2,1)} %broadcast_in_dim.32), calls=%async_computation.2 | async-start | bytes 4194304 | tf_op jit(solution)/shard_map/all_to_all | solution.py:33
  318.8 7.1 %copy-start.4 = (f32[3,704]{1,0:T(4,128)S(1)}, f32[3,704]{1,0:T(4,128)}, u32[]{:S(2)}) copy-start(f32[3,704]{1,0:T(4,128)} %param.25) | copy-start | bytes 25348
  322.4 10.4 %copy-start.7 = (f32[704]{0:T(1024)S(1)}, f32[704]{0:T(1024)}, u32[]{:S(2)}) copy-start(f32[704]{0:T(1024)} %param.26) | copy-start | bytes 8452
  322.5 4.8 %collective-permute-start = (bf16[1,704]{0,1:T(8,128)(2,1)S(1)}, bf16[1,704]{0,1:T(8,128)(2,1)S(1)}, u32[]{:S(2)}, u32[]{:S(2)}) collective-permute-start(bf16[1,704]{0,1:T(8,128)(2,1)S(1)} %get-tuple-element.120), channel_id=1, source_target_pairs={{0,8},{8,16},{16,24},{24,32},{32,40},{40,48},{48,56},{56,64},{64,7... | collective-permute-start | bytes 4232 | tf_op jit(solution)/shard_map/ppermute | solution.py:60
  324.4 6.8 %collective-permute-start.1 = (bf16[1,704]{0,1:T(8,128)(2,1)S(1)}, bf16[1,704]{0,1:T(8,128)(2,1)S(1)}, u32[]{:S(2)}, u32[]{:S(2)}) collective-permute-start(bf16[1,704]{0,1:T(8,128)(2,1)S(1)} %get-tuple-element.121), channel_id=1, source_target_pairs={{8,0},{16,8},{24,16},{32,24},{40,32},{48,40},{56,48},{64,56},{72,6... | collective-permute-start | bytes 4232 | tf_op jit(solution)/shard_map/ppermute | solution.py:62
Sparse Core Ops, SparseCore 0:
  9.9 101.0 all-gather.4
  112.8 42.2 all-gather.6
  156.8 43.6 all-gather.10
  202.1 43.5 all-gather.8
where the time goes:
time: 386 us; the launch traced here: 383 us
  waiting for transfers between devices  112 us (29%)
  matrix products  101 us (26%)
  blocking collectives  75.1 us (19%)
  local copies, waits for them, and re-layouts  52.3 us (14%)
  other arithmetic  15.7 us (4%)
  between operations  14 us (4%)
  starting transfers between devices  13.3 us (3%)
    all_gather x1, waiting for transfers between devices, sent_together(): lax.all_gather(both, axis, axis=dim, tiled=True)  65.2 us
    dot_general x8, matrix products, advance(): jnp.einsum('qhmd,khmd->hmqk', query_heads, key_block, preferred_element_t...  44.5 us
    dot_general x8, matrix products, advance(): jnp.einsum('hmqk,khe->hmqe', shifted.astype(jnp.bfloat16), value_block, p...  42.3 us
    all_to_all x2, waiting for transfers between devices, sent_to_all(): return lax.all_to_all(copies, axis, split_axis=0, concat_axis=0, tiled=True)  41 us
    all_gather x3, blocking collectives, whole_of(): nearer = lax.all_gather(array, axes[-1], axis=dim, tiled=True)  36.4 us
    all_to_all x1, blocking collectives, sent_and_summed(): lax.all_to_all(split_up(array, dim, devices), axis, 0, 0, tiled=True)  30.7 us
    unnamed x17, local copies, waits for them, and re-layouts  20.5 us
    reshape x1, local copies, waits for them, and re-layouts, on_device(): key_blocks = key_rows.reshape(count // block, block, heads, 2, HD)  14.7 us
  transfers between devices with their start and end apart: 8, of which 5 were waited for; matrix products, arithmetic and copies ran while one was open for 39% of the time, Pallas kernels for 0%

commit v1 on v0

v1 whole, which is shorter than its diff:
```python
import functools

import jax
import jax.numpy as jnp
from jax import lax
from jax.experimental import pallas as pl
from jax.experimental.pallas import tpu as pltpu
from jax.sharding import PartitionSpec as P

D = 2048
HD = 64
VD = 128
LOG2E = 1.4426950408889634
NZ = 8
NY = 4
F32 = jnp.float32
BF16 = jnp.bfloat16
MESH = pl.DeviceIdType.MESH
VMEM = pl.BlockSpec(memory_space=pltpu.VMEM)
ANY = pl.BlockSpec(memory_space=pl.ANY)


def remote(src, dst, send, recv, device):
    return pltpu.make_async_remote_copy(
        src_ref=src, dst_ref=dst, send_sem=send, recv_sem=recv, device_id=device, device_id_type=MESH
    )


def meet(peers):
    barrier = pltpu.get_barrier_semaphore()
    for peer in peers:
        pl.semaphore_signal(barrier, inc=1, device_id=peer, device_id_type=MESH)
    pl.semaphore_wait(barrier, len(peers))


def attention_kernel(
    q_ref,
    k_ref,
    v_ref,
    gu_ref,
    lam_ref,
    gain_ref,
    out_ref,
    gug,
    kbuf,
    vbuf,
    qbuf,
    kk,
    vv,
    qbd,
    top,
    total,
    acc,
    osend,
    ssend,
    orecv,
    srecv,
    ks,
    kr,
    vs,
    vr,
    qs,
    qr,
    gs,
    gr,
    ya_s,
    ya_r,
    yb_s,
    yb_r,
    os,
    orr,
    ss,
    sr,
    loc,
):
    sp, tp = lax.axis_index("sp"), lax.axis_index("tp")
    z, y = sp // NY, sp % NY
    length = q_ref.shape[0]
    cols = 2 * length
    half = length // 2
    rows_g = gu_ref.shape[0]
    hg = rows_g // 2

    def index(dz, dy):
        return ((z + dz) % NZ) * NY + (y + dy) % NY

    def device(dz, dy):
        return (index(dz % NZ, dy % NY), tp)

    zr, zl = device(1, 0), device(7, 0)
    yr, yl = device(0, 1), device(0, 3)
    meet([zr, zl, yr, yl, device(0, 2)])
    started = []

    def go(copy):
        copy.start()
        started.append(copy)
        return copy

    def kslot(s):
        return k_ref if s == 0 else kbuf.at[s]

    def vslot(s):
        return v_ref if s == 0 else vbuf.at[s]

    def gslot(s, rows=None):
        if s == 0:
            return gu_ref if rows is None else gu_ref.at[rows]
        whole = gug.at[index(8 - s, 0)]
        return whole if rows is None else whole.at[rows]

    qa = [
        go(remote(q_ref, qbuf.at[1], qs.at[0], qr.at[0], yr)),
        go(remote(q_ref, qbuf.at[3], qs.at[1], qr.at[1], yl)),
    ]

    def send_kv(t):
        right, left = t, (8 - t) % 8
        out = []
        out.append(go(remote(kslot(right), kbuf.at[t + 1], ks.at[0, t], kr.at[t + 1], zr)))
        if t < 3:
            out.append(go(remote(kslot(left), kbuf.at[7 - t], ks.at[1, t], kr.at[7 - t], zl)))
            out.append(go(remote(vslot(right), vbuf.at[t + 1], vs.at[0, t], vr.at[t + 1], zr)))
        out.append(go(remote(vslot(left), vbuf.at[7 - t], vs.at[1, t], vr.at[7 - t], zl)))
        return out

    def send_g(t):
        right, left = t, (8 - t) % 8
        dst_r, dst_l = gug.at[index(8 - right, 0)], gug.at[index(8 - left, 0)]
        if t < 3:
            return [
                go(remote(gslot(right), dst_r, gs.at[0, t], gr.at[0, t], zr)),
                go(remote(gslot(left), dst_l, gs.at[1, t], gr.at[1, t], zl)),
            ]
        top_half, low_half = pl.ds(0, hg), pl.ds(hg, hg)
        return [
            go(remote(gslot(right, top_half), dst_r.at[top_half], gs.at[0, t], gr.at[0, t], zr)),
            go(remote(gslot(left, low_half), dst_l.at[low_half], gs.at[1, t], gr.at[1, t], zl)),
        ]

    def send_ya(s):
        dst = gug.at[index(8 - s, 0)]
        return [
            go(remote(gslot(s), dst, ya_s.at[0, s], ya_r.at[0, s], yr)),
            go(remote(gslot(s), dst, ya_s.at[1, s], ya_r.at[1, s], yl)),
        ]

    def send_yb(s):
        top_half, low_half = pl.ds(0, hg), pl.ds(hg, hg)
        a = gug.at[index(8 - s, 3)].at[top_half]
        b = gug.at[index(8 - s, 1)].at[low_half]
        return [
            go(remote(a, a, yb_s.at[0, s], yb_r.at[0, s], yr)),
            go(remote(b, b, yb_s.at[1, s], yb_r.at[1, s], yl)),
        ]

    def arrive(copies):
        for copy in copies:
            copy.wait_recv()

    kv = [send_kv(0)]
    g = [send_g(0)]
    own = pltpu.make_async_copy(gu_ref, gug.at[sp], loc)
    own.start()
    ya = {0: send_ya(0)}
    yb = {}

    top[...] = jnp.full(top.shape, -1e30, F32)
    total[...] = jnp.zeros(total.shape, F32)
    acc[...] = jnp.zeros(acc.shape, F32)
    row = lax.broadcasted_iota(jnp.int32, (2 * HD, 128), 0)

    def lay_queries(src, slot):
        for j in range(length // 128):
            turned = src[j * 128 : (j + 1) * 128, :].astype(F32).T * (LOG2E * HD**-0.5)
            for m in range(2):
                at = slot * cols + j * 256 + m * 128
                kept = jnp.where((row < HD) if m == 0 else (row >= HD), turned, 0.0)
                high = kept.astype(BF16)
                qbd[0:128, at : at + 128] = high
                qbd[128:256, at : at + 128] = (kept - high.astype(F32)).astype(BF16)

    def stage(slots):
        for n, s in enumerate(slots):
            kb = kslot(s)[...]
            kk[n * length : (n + 1) * length, 0:128] = kb
            kk[n * length : (n + 1) * length, 128:256] = kb
            vv[n * length : (n + 1) * length, :] = vslot(s)[...]

    def attend(count, first, last):
        keys = count * length

        def tile(i, carry):
            at = pl.ds(pl.multiple_of(i * cols, cols), cols)
            scores = jnp.dot(kk[0:keys, :], qbd[:, at], preferred_element_type=F32)
            before = top[0:1, at]
            now = jnp.maximum(before, jnp.max(scores, axis=0, keepdims=True))
            shifted = jnp.exp2(scores - now)
            factor = jnp.exp2(before - now)
            top[0:1, at] = now
            total[0:1, at] = total[0:1, at] * factor + jnp.sum(shifted, axis=0, keepdims=True)
            acc[:, at] = acc[:, at] * factor + lax.dot_general(
                vv[0:keys, :],
                shifted.astype(BF16),
                (((0,), (0,)), ((), ())),
                preferred_element_type=F32,
            )
            return carry

        lax.fori_loop(first, last, tile, 0)

    lay_queries(q_ref, 0)
    stage([0])
    attend(1, 0, 1)
    arrive(qa)
    qb = [
        go(remote(qbuf.at[1, pl.ds(0, half)], qbuf.at[2, pl.ds(0, half)], qs.at[2], qr.at[2], yr)),
        go(remote(qbuf.at[3, pl.ds(half, half)], qbuf.at[2, pl.ds(half, half)], qs.at[3], qr.at[3], yl)),
    ]
    lay_queries(qbuf.at[1], 1)
    lay_queries(qbuf.at[3], 3)
    attend(1, 1, 2)
    attend(1, 3, 4)
    arrive(qb)
    lay_queries(qbuf.at[2], 2)
    attend(1, 2, 3)

    for t in range(1, 5):
        arrive(kv[t - 1])
        if t < 4:
            kv.append(send_kv(t))
        arrive(g[t - 1])
        if t < 4:
            g.append(send_g(t))
        slots = [t, 8 - t] if t < 4 else [4]
        for s in slots:
            ya[s] = send_ya(s)
        if t == 1:
            arrive(ya[0])
            yb[0] = send_yb(0)
        else:
            for s in (t - 1, 9 - t):
                arrive(ya[s])
                yb[s] = send_yb(s)
        stage(slots)
        attend(len(slots), 0, 4)

    sent = []
    for slot in (2, 1, 3):
        at = slice(slot * cols, (slot + 1) * cols)
        scale = 1.0 / total[0:1, at]
        osend[slot] = (acc[:, at] * scale).astype(BF16)
        ssend[slot, 0:1, :] = top[0:1, at]
        ssend[slot, 1:2, :] = total[0:1, at]
        ssend[slot, 2:8, :] = jnp.zeros((6, cols), F32)
        to = device(0, 4 - slot)
        sent.append(go(remote(osend.at[slot], orecv.at[slot], os.at[slot], orr.at[slot], to)))
        sent.append(go(remote(ssend.at[slot], srecv.at[slot], ss.at[slot], sr.at[slot], to)))
    arrive(ya[4])
    yb[4] = send_yb(4)
    arrive(sent)

    tops = [top[0:1, 0:cols]] + [srecv[s, 0:1, :] for s in (1, 2, 3)]
    sums = [total[0:1, 0:cols]] + [srecv[s, 1:2, :] for s in (1, 2, 3)]
    highest = jnp.maximum(jnp.maximum(tops[0], tops[1]), jnp.maximum(tops[2], tops[3]))
    shares = [jnp.exp2(m - highest) for m in tops]
    whole = sum(s * w for s, w in zip(sums, shares))
    inverse = 1.0 / whole
    weights = [shares[0] * inverse] + [shares[s] * sums[s] * inverse for s in (1, 2, 3)]
    for j in range(length // 128):
        maps = []
        for m in range(2):
            at = slice(j * 256 + m * 128, j * 256 + (m + 1) * 128)
            value = acc[:, at] * weights[0][:, at]
            for s in (1, 2, 3):
                value = value + orecv[s, :, at].astype(F32) * weights[s][:, at]
            maps.append(value)
        mixed = maps[0] - lam_ref[0:1, :] * maps[1]
        spread = jnp.mean(mixed * mixed, axis=0, keepdims=True)
        normed = mixed * lax.rsqrt(spread + 1e-06)
        out_ref[j * 128 : (j + 1) * 128, :] = (normed.T * gain_ref[0:1, :] * 0.8).astype(BF16)

    for s in range(8):
        arrive(yb[s])
    for copy in started:
        copy.wait_send()
    own.wait()


def attention(q, k, v, gu, lam, gain):
    length = q.shape[0]
    cols = 2 * length
    dma = pltpu.SemaphoreType.DMA
    return pl.pallas_call(
        attention_kernel,
        name="attention",
        out_shape=(
            jax.ShapeDtypeStruct((length, VD), BF16),
            jax.ShapeDtypeStruct((NZ * NY, *gu.shape), BF16),
        ),
        in_specs=[VMEM] * 6,
        out_specs=(VMEM, ANY),
        scratch_shapes=[
            pltpu.VMEM((8, length, 128), BF16),
            pltpu.VMEM((8, length, 128), BF16),
            pltpu.VMEM((4, length, 128), BF16),
            pltpu.VMEM((2 * length, 256), BF16),
            pltpu.VMEM((2 * length, 128), BF16),
            pltpu.VMEM((256, 4 * cols), BF16),
            pltpu.VMEM((8, 4 * cols), F32),
            pltpu.VMEM((8, 4 * cols), F32),
            pltpu.VMEM((VD, 4 * cols), F32),
            pltpu.VMEM((4, VD, cols), BF16),
            pltpu.VMEM((4, 8, cols), F32),
            pltpu.VMEM((4, VD, cols), BF16),
            pltpu.VMEM((4, 8, cols), F32),
            dma((2, 4)),
            dma((8,)),
            dma((2, 4)),
            dma((8,)),
            dma((4,)),
            dma((4,)),
            dma((2, 4)),
            dma((2, 4)),
            dma((2, 8)),
            dma((2, 8)),
            dma((2, 8)),
            dma((2, 8)),
            dma((4,)),
            dma((4,)),
            dma((4,)),
            dma((4,)),
            dma,
        ],
        compiler_params=pltpu.CompilerParams(
            collective_id=0, has_side_effects=True, vmem_limit_bytes=60 * 2**20
        ),
    )(q, k, v, gu, lam, gain)


def tail_kernel(
    heads_ref,
    resid_ref,
    ow_ref,
    ng_ref,
    cw_ref,
    cb_ref,
    dw_ref,
    gug,
    out_ref,
    hall,
    nall,
    am,
    ssq,
    gu,
    big,
    gpad,
    gedge,
    halo,
    hid,
    dall,
    psib,
    rsib,
    pout,
    rout,
    xs,
    xr,
    cs,
    cr,
    ts,
    tr,
    es,
    er,
    ys,
    yrr,
    zs,
    zrr,
    bs,
    br,
    ps,
    pr,
    loc,
):
    sp, tp = lax.axis_index("sp"), lax.axis_index("tp")
    z, y = sp // NY, sp % NY
    x, c = tp // 2, tp % 2
    length = heads_ref.shape[0]
    half = length // 2
    width = resid_ref.shape[1]
    units = dw_ref.shape[1]
    hg = dw_ref.shape[0] // 2

    def xdev(dx, other=0):
        return (sp, ((x + dx) % 4) * 2 + (c + other) % 2)

    def index(dz, dy):
        return ((z + dz) % NZ) * NY + (y + dy) % NY

    def device(dz, dy):
        return (index(dz, dy), tp)

    xr_, xl_, sib = xdev(1), xdev(3), xdev(0, 1)
    zr, zl = device(1, 0), device(7, 0)
    after, before = ((sp + 1) % (NZ * NY), tp), ((sp + NZ * NY - 1) % (NZ * NY), tp)
    tp_peers = [(sp, (tp + i) % 8) for i in range(1, 8)]
    meet(tp_peers + [after, before, zr, zl] + [device(0, i) for i in (1, 2, 3)])
    started = []

    def go(copy):
        copy.start()
        started.append(copy)
        return copy

    def arrive(copies):
        for copy in copies:
            copy.wait_recv()

    load = pltpu.make_async_copy(gug, gu, loc)
    load.start()

    dy = [
        go(remote(dw_ref, dall.at[sp], ys.at[i], yrr.at[i], device(0, i))) for i in (1, 2, 3)
    ]
    dall[sp] = dw_ref[...]

    def dcol(dz):
        return pl.ds(((z + dz) % NZ) * NY, NY)

    def send_d(t):
        right, left = dcol(8 - t), dcol(t)
        if t == 3:
            right = pl.ds(((z + 8 - t) % NZ) * NY, NY // 2)
            left = pl.ds(((z + t) % NZ) * NY + NY // 2, NY // 2)
        return [
            go(remote(dall.at[right], dall.at[right], zs.at[0, t], zrr.at[0, t], zr)),
            go(remote(dall.at[left], dall.at[left], zs.at[1, t], zrr.at[1, t], zl)),
        ]

    def gather(stack, k):
        mine = stack.at[tp]
        one = [
            go(remote(mine, mine, xs.at[k, 0], xr.at[k, 0], xr_)),
            go(remote(mine, mine, xs.at[k, 1], xr.at[k, 1], xl_)),
        ]
        core = [go(remote(mine, mine, cs.at[k, 0], cr.at[k, 0], sib))]
        arrive(core)
        yield 0
        from_left = stack.at[((x + 3) % 4) * 2 + c]
        from_right = stack.at[((x + 1) % 4) * 2 + c]
        upper, lower = pl.ds(0, half), pl.ds(half, half)
        arrive(one[:1])
        two = [go(remote(from_left.at[upper], from_left.at[upper], xs.at[k, 2], xr.at[k, 2], xr_))]
        core.append(go(remote(from_left, from_left, cs.at[k, 1], cr.at[k, 1], sib)))
        arrive(one[1:])
        two.append(go(remote(from_right.at[lower], from_right.at[lower], xs.at[k, 3], xr.at[k, 3], xl_)))
        core.append(go(remote(from_right, from_right, cs.at[k, 2], cr.at[k, 2], sib)))
        arrive(core[1:2])
        yield 3
        arrive(core[2:3])
        yield 1
        far = stack.at[((x + 2) % 4) * 2 + c]
        arrive(two[:1])
        core.append(go(remote(far.at[upper], far.at[upper], cs.at[k, 3], cr.at[k, 3], sib)))
        arrive(two[1:])
        core.append(go(remote(far.at[lower], far.at[lower], cs.at[k, 4], cr.at[k, 4], sib)))
        arrive(core[3:5])
        yield 2

    hall[tp] = heads_ref[...]
    am[...] = resid_ref[...].astype(F32)
    for dx in gather(hall, 0):
        chip = (x + dx) % 4
        for core in range(2):
            rows = pl.ds(pl.multiple_of((chip * 2 + core) * VD, VD), VD)
            am[...] += jnp.dot(hall[chip * 2 + core], ow_ref[rows, :], preferred_element_type=F32)
    value = am[...]
    nall[tp] = (value * ng_ref[0:1, :]).astype(BF16)
    square = value * value
    square = square[:, 0:128] + square[:, 128:256]
    for j in range(length // 128):
        part = jnp.sum(square[j * 128 : (j + 1) * 128, :].T, axis=0, keepdims=True)
        ssq[tp, 0:8, j * 128 : (j + 1) * 128] = jnp.broadcast_to(part, (8, 128))

    arrive(dy)
    dz = [send_d(0)]
    load.wait()
    tiny = []

    def product(chip):
        a = jnp.concatenate([nall[chip * 2], nall[chip * 2 + 1]], axis=1)
        rows = pl.ds(pl.multiple_of(chip * 2 * width, 2 * width), 2 * width)
        return jnp.dot(a, gu[rows, :], preferred_element_type=F32)

    for n, dx in enumerate(gather(nall, 1)):
        if n == 0:
            tiny = [
                go(remote(ssq.at[tp], ssq.at[tp], ts.at[i - 1], tr.at[i - 1], (sp, (tp + i) % 8)))
                for i in range(1, 8)
            ]
            big[...] = product((x + dx) % 4)
        else:
            if n == 2:
                arrive(dz[0])
                dz.append(send_d(1))
            big[...] += product((x + dx) % 4)
    arrive(dz[1])
    dz.append(send_d(2))
    arrive(tiny)
    squares = sum(ssq[i, 0:1, :] for i in range(8))
    factor = lax.rsqrt(squares * (1.0 / D) + 1e-06)
    whole = units // 128 * 128
    rest = units - whole
    for j in range(length // 128):
        rows = slice(j * 128, (j + 1) * 128)
        column = jnp.broadcast_to(factor[:, rows], (128, 128)).T[:, 0:1]
        scaled = big[rows, :] * column
        gate = jnp.concatenate([scaled[:, 0:whole], scaled[:, 2 * whole : 2 * whole + rest]], axis=1)
        gpad[8 + j * 128 : 8 + (j + 1) * 128, :] = gate.astype(BF16).astype(F32)
        big[rows, whole:] = scaled[:, whole:]
    gedge[0] = gpad[8:24, :].astype(BF16)
    gedge[1] = gpad[8 + length - 16 : 8 + length, :].astype(BF16)
    edge = [
        go(remote(gedge.at[1], halo.at[0], es.at[0], er.at[0], after)),
        go(remote(gedge.at[0], halo.at[1], es.at[1], er.at[1], before)),
    ]
    arrive(edge)
    previous = jnp.where(sp == 0, 0.0, halo[0].astype(F32)[15:16, :])
    following = jnp.where(sp == NZ * NY - 1, 0.0, halo[1].astype(F32)[0:1, :])
    gpad[7:8, :] = previous
    gpad[8 + length : 9 + length, :] = following
    for j in range(length // 128):
        rows = slice(j * 128, (j + 1) * 128)
        at = 8 + j * 128
        conv = (
            gpad[at - 1 : at + 127, :] * cw_ref[0:1, :]
            + gpad[at : at + 128, :] * cw_ref[1:2, :]
            + gpad[at + 1 : at + 129, :] * cw_ref[2:3, :]
            + cb_ref[0:1, :]
        )
        up = jnp.concatenate([big[rows, whole : 2 * whole], big[rows, 2 * whole + rest :]], axis=1)
        hid[rows, :] = (conv / (1.0 + jnp.exp(-conv)) * up).astype(BF16)

    arrive(dz[2])
    dz.append(send_d(3))
    arrive(dz[3])
    per = width // dw_ref.shape[0]

    def down(target):
        w = dall[pl.ds(target * per, per)].reshape(width, units)
        return lax.dot_general(
            hid[...], w, (((1,), (1,)), ((), ())), preferred_element_type=F32
        )

    order = (2, 1, 3, 0)
    for dx in order:
        psib[dx] = down(((x + dx) % 4) * 2 + (1 - c)).astype(BF16)
        go(remote(psib.at[dx], rsib.at[dx], bs.at[dx], br.at[dx], sib))
    final = []
    for dx in order:
        piece = down(((x + dx) % 4) * 2 + c)
        remote(psib.at[dx], rsib.at[dx], bs.at[dx], br.at[dx], sib).wait_recv()
        piece = piece + rsib[dx].astype(F32)
        if dx == 0:
            am[...] += piece
        else:
            pout[dx] = piece.astype(BF16)
            final.append(go(remote(pout.at[dx], rout.at[dx], ps.at[dx], pr.at[dx], xdev(dx))))
    arrive(final)
    out_ref[...] = (
        am[...] + (rout[1].astype(F32) + rout[2].astype(F32) + rout[3].astype(F32))
    ).astype(BF16)
    for copy in started:
        copy.wait_send()


def tail(heads, resid, ow, ng, cw, cb, dw, gug):
    length, width = resid.shape
    units = dw.shape[1]
    dma = pltpu.SemaphoreType.DMA
    return pl.pallas_call(
        tail_kernel,
        name="tail",
        out_shape=jax.ShapeDtypeStruct((length, width), BF16),
        in_specs=[VMEM] * 7 + [ANY],
        out_specs=VMEM,
        scratch_shapes=[
            pltpu.VMEM((8, length, VD), BF16),
            pltpu.VMEM((8, length, width), BF16),
            pltpu.VMEM((length, width), F32),
            pltpu.VMEM((8, 8, length), F32),
            pltpu.VMEM(gug.shape, BF16),
            pltpu.VMEM((length, 2 * units), F32),
            pltpu.VMEM((length + 16, units), F32),
            pltpu.VMEM((2, 16, units), BF16),
            pltpu.VMEM((2, 16, units), BF16),
            pltpu.VMEM((length, units), BF16),
            pltpu.VMEM((NZ * NY, *dw.shape), BF16),
            pltpu.VMEM((4, length, width), BF16),
            pltpu.VMEM((4, length, width), BF16),
            pltpu.VMEM((4, length, width), BF16),
            pltpu.VMEM((4, length, width), BF16),
            dma((2, 4)),
            dma((2, 4)),
            dma((2, 5)),
            dma((2, 5)),
            dma((7,)),
            dma((7,)),
            dma((2,)),
            dma((2,)),
            dma((4,)),
            dma((4,)),
            dma((2, 4)),
            dma((2, 4)),
            dma((4,)),
            dma((4,)),
            dma((4,)),
            dma((4,)),
            dma,
        ],
        compiler_params=pltpu.CompilerParams(
            collective_id=1, has_side_effects=True, vmem_limit_bytes=60 * 2**20
        ),
    )(heads, resid, ow, ng, cw, cb, dw, gug)


def on_device(
    resid,
    queries,
    keys,
    values,
    mix_lambda,
    head_gain,
    out_weight,
    norm_gain,
    gate_weight,
    up_weight,
    conv_weight,
    conv_bias,
    down_weight,
):
    units = gate_weight.shape[1]
    whole = units // 128 * 128
    gu = jnp.concatenate(
        [gate_weight[:, :whole], up_weight[:, :whole], gate_weight[:, whole:], up_weight[:, whole:]], axis=1
    )
    lam = jnp.broadcast_to(mix_lambda.reshape(1, 1), (8, 128))
    gain = jnp.broadcast_to(head_gain[None, :], (8, VD))
    heads_out, gug = attention(queries, keys, values, gu, lam, gain)
    return tail(
        heads_out,
        resid,
        out_weight,
        norm_gain[None, :],
        conv_weight,
        conv_bias[None, :],
        down_weight.T,
        gug.reshape(-1, gug.shape[-1]),
    )


def solution(mesh):
    return jax.shard_map(
        on_device,
        mesh=mesh,
        in_specs=(
            P("sp", "tp"),
            P("sp", "tp"),
            P("sp", "tp"),
            P("sp", "tp"),
            P("tp"),
            P(),
            P(None, "tp"),
            P("tp"),
            P("sp", "tp"),
            P("sp", "tp"),
            P(None, "tp"),
            P("tp"),
            P("tp", "sp"),
        ),
        out_specs=P("sp", "tp"),
        check_vma=False,
    )
```

time: 386 us -> 162 us (0.42)
  Pallas kernels: 0 us -> 153 us
  waiting for transfers between devices: 112 us -> 0 us
  matrix products: 101 us -> 0 us
  blocking collectives: 75.1 us -> 0 us
  local copies, waits for them, and re-layouts: 52.3 us -> 8.77 us
  other arithmetic: 15.7 us -> 0 us
  between operations: 14 us -> 0.67 us
  starting transfers between devices: 13.3 us -> 0 us
    pallas_call x0 -> x2, Pallas kernels: none -> 153 us  [the longest x1 78.7 us: attention(): pl.pallas_call(attention_kernel, name='attention', out_shape=(jax.ShapeDt...]
    dot_general x19 -> x0, matrix products: 101 us -> none  [the longest x8 44.5 us: advance(): jnp.einsum('qhmd,khmd->hmqk', query_heads, key_block, preferred_element_t...]
    all_gather x4 -> x0, waiting for transfers between devices: 65.2 us -> none  [the longest x1 65.2 us: sent_together(): lax.all_gather(both, axis, axis=dim, tiled=True)]
    all_to_all x2 -> x0, waiting for transfers between devices: 41 us -> none  [sent_to_all(): return lax.all_to_all(copies, axis, split_axis=0, concat_axis=0, tiled=True)]
    all_to_all x2 -> x0, blocking collectives: 38.7 us -> none  [the longest x1 30.7 us: sent_and_summed(): lax.all_to_all(split_up(array, dim, devices), axis, 0, 0, tiled=True)]
    all_gather x3 -> x0, blocking collectives: 36.4 us -> none  [whole_of(): nearer = lax.all_gather(array, axes[-1], axis=dim, tiled=True)]
    unnamed x17 -> x1, local copies, waits for them, and re-layouts: 20.5 us -> 1.67 us
    reshape x2 -> x0, local copies, waits for them, and re-layouts: 16.5 us -> none  [the longest x1 14.7 us: on_device(): key_blocks = key_rows.reshape(count // block, block, heads, 2, HD)]
  transfers between devices with their start and end apart: 8 -> 0, of which waited for: 5 -> 0; matrix products, arithmetic and copies ran while one was open for 39% -> 0% of each run, Pallas kernels for 0% -> 0%
where the time goes in v1:
time: 162 us
  Pallas kernels  153 us (94%)
  local copies, waits for them, and re-layouts  8.77 us (5%)
    pallas_call x1, Pallas kernels, attention(): pl.pallas_call(attention_kernel, name='attention', out_shape=(jax.ShapeDt...  78.7 us
    pallas_call x1, Pallas kernels, tail(): pl.pallas_call(tail_kernel, name='tail', out_shape=jax.ShapeDtypeStruct((...  74 us

profile of v1, /device:TPU:1, one launch (start us, length us, event | category | flops | bytes accessed | tf_op | source)
XLA Modules:
  0.0 162.0 jit_solution(15987431601573771649)
XLA Ops:
  0.7 1.3 broadcast_in_dim.23.cb_ref
  1.9 0.6 broadcast_in_dim.20.lam_ref
  2.5 1.2 broadcast_in_dim.21.gain_ref
  3.8 0.7 slice.14
  4.5 0.7 slice.15
  5.2 0.9 slice.12
  6.1 0.9 slice.13
  7.0 0.8 concatenate.3.gu_ref
  7.8 78.7 %attention.1 = (bf16[512,128]{1,0:T(8,128)(2,1)}, bf16[32,64,1408]{2,1,0:T(8,128)(2,1)}) custom-call(bf16[512,128]{1,0:T(8,128)(2,1)} %q_ref.1, bf16[512,128]{1,0:T(8,128)(2,1)} %k_ref.1, bf16[512,128]{1,0:T(8,128)(2,1)} %v_ref.1, bf16[64,1408]{1,0:T(8,128)(2,1)} %concatenate.3.gu_ref, f32[8,128]{1,0:T(8,128)} %broadcast_in_dim.20.lam_ref, ...), custom_call_target="tpu_custom_call" | custom-call | tf_op jit(solution)/shard_map/attention/pallas_call | solution.py:294
  86.4 74.0 %tail.1 = bf16[512,256]{1,0:T(8,128)(2,1)} custom-call(bf16[512,128]{1,0:T(8,128)(2,1)} %get-tuple-element.7.heads_ref, bf16[512,256]{1,0:T(8,128)(2,1)} %resid_ref.1, bf16[1024,256]{1,0:T(8,128)(2,1)} %ow_ref.1, f32[1,256]{1,0:T(1,128)} %bitcast.7, f32[3,704]{1,0:T(4,128)} %cw_ref.1, f32[1,704]{1,0:T(1,128)} %broadcast_in_dim.23.cb_ref, ...), custom_call_target="tpu_custom_call" | custom-call | tf_op jit(solution)/shard_map/tail/pallas_call | solution.py:580
  160.4 1.7 %copy.16 = bf16[512,256]{1,0:T(8,128)(2,1)} copy(bf16[512,256]{1,0:T(8,128)(2,1)} %tail.1) | data formatting | bytes 524288

commit v2 on v1

v2 whole, which is shorter than its diff:
```python
import functools

import jax
import jax.numpy as jnp
from jax import lax
from jax.experimental import pallas as pl
from jax.experimental.pallas import tpu as pltpu
from jax.sharding import PartitionSpec as P

D = 2048
HD = 64
VD = 128
LOG2E = 1.4426950408889634
NZ = 8
NY = 4
F32 = jnp.float32
BF16 = jnp.bfloat16
MESH = pl.DeviceIdType.MESH
VMEM = pl.BlockSpec(memory_space=pltpu.VMEM)
ANY = pl.BlockSpec(memory_space=pl.ANY)
SMEM = pl.BlockSpec(memory_space=pltpu.SMEM)


def remote(src, dst, send, recv, device):
    return pltpu.make_async_remote_copy(
        src_ref=src, dst_ref=dst, send_sem=send, recv_sem=recv, device_id=device, device_id_type=MESH
    )


def meet(peers):
    barrier = pltpu.get_barrier_semaphore()
    for peer in peers:
        pl.semaphore_signal(barrier, inc=1, device_id=peer, device_id_type=MESH)
    pl.semaphore_wait(barrier, len(peers))


def attention_kernel(
    q_ref,
    k_ref,
    v_ref,
    gate_ref,
    up_ref,
    lam_ref,
    gain_ref,
    out_ref,
    gug,
    guo,
    kbuf,
    vbuf,
    qbuf,
    kk,
    vv,
    qbd,
    top,
    total,
    acc,
    lse,
    part,
    relay,
    landed,
    ks,
    kr,
    vs,
    vr,
    qs,
    qr,
    gs,
    gr,
    ya_s,
    ya_r,
    yb_s,
    yb_r,
    hs,
    hr,
    hz_s,
    hz_r,
    ls,
    lr,
    ms,
    mr,
    loc,
):
    sp, tp = lax.axis_index("sp"), lax.axis_index("tp")
    z, y = sp // NY, sp % NY
    length = q_ref.shape[0]
    cols = 2 * length
    half = length // 2
    units = gate_ref.shape[1]
    whole = units // 128 * 128
    rest = units - whole
    first = pl.ds(0, 48)
    last = pl.ds(48, 16)

    def index(dz, dy):
        return ((z + dz) % NZ) * NY + (y + dy) % NY

    def device(dz, dy):
        return (index(dz, dy), tp)

    zr, zl = device(1, 0), device(7, 0)
    yr, yl = device(0, 1), device(0, 3)
    guo[:, 0:whole] = gate_ref[:, 0:whole]
    guo[:, whole : 2 * whole] = up_ref[:, 0:whole]
    guo[:, 2 * whole :] = jnp.concatenate([gate_ref[:, whole:], up_ref[:, whole:]], axis=1)
    meet([zr, zl, yr, yl, device(0, 2)])
    started = []

    def go(copy):
        copy.start()
        started.append(copy)
        return copy

    def arrive(copies):
        for copy in copies:
            copy.wait_recv()

    def kslot(s):
        return k_ref if s == 0 else kbuf.at[s]

    def vslot(s):
        return v_ref if s == 0 else vbuf.at[s]

    def send_kv(t):
        right, left = t, (8 - t) % 8
        out = [go(remote(kslot(right), kbuf.at[t + 1], ks.at[0, t], kr.at[t + 1], zr))]
        if t < 3:
            out.append(go(remote(kslot(left), kbuf.at[7 - t], ks.at[1, t], kr.at[7 - t], zl)))
            out.append(go(remote(vslot(right), vbuf.at[t + 1], vs.at[0, t], vr.at[t + 1], zr)))
        out.append(go(remote(vslot(left), vbuf.at[7 - t], vs.at[1, t], vr.at[7 - t], zl)))
        return out

    def source(s, rows):
        return guo.at[rows] if s == 0 else gug.at[index(8 - s, 0), rows]

    def parts(s):
        return (pl.ds(0, 16), pl.ds(16, 32)) if s % 2 == 0 else (pl.ds(0, 32), pl.ds(32, 16))

    def send_g(t):
        right, left = t, (8 - t) % 8
        rows_r, rows_l = parts(0) if t == 3 else (first, first)
        return [
            go(remote(source(right, rows_r), gug.at[index(8 - right, 0), rows_r], gs.at[0, t], gr.at[0, t], zr)),
            go(remote(source(left, rows_l), gug.at[index(8 - left, 0), rows_l], gs.at[1, t], gr.at[1, t], zl)),
        ]

    def send_ya(s):
        dst = gug.at[index(8 - s, 0), first]
        return [
            go(remote(source(s, first), dst, ya_s.at[0, s], ya_r.at[0, s], yr)),
            go(remote(source(s, first), dst, ya_s.at[1, s], ya_r.at[1, s], yl)),
        ]

    def send_yb(s):
        rows_r, rows_l = parts(s)
        a = gug.at[index(8 - s, 3), rows_r]
        b = gug.at[index(8 - s, 1), rows_l]
        return [
            go(remote(a, a, yb_s.at[0, s], yb_r.at[0, s], yr)),
            go(remote(b, b, yb_s.at[1, s], yb_r.at[1, s], yl)),
        ]

    def send_h(t):
        right, left = ((z + 8 - t) % NZ) * NY, ((z + t) % NZ) * NY
        if t < 3:
            a, b = gug.at[pl.ds(right, NY), last], gug.at[pl.ds(left, NY), last]
        else:
            a, b = gug.at[pl.ds(right, 2), last], gug.at[pl.ds(left + 2, 2), last]
        return [
            go(remote(a, a, hz_s.at[0, t], hz_r.at[0, t], zr)),
            go(remote(b, b, hz_s.at[1, t], hz_r.at[1, t], zl)),
        ]

    qa = [
        go(remote(q_ref, qbuf.at[1], qs.at[0], qr.at[0], yr)),
        go(remote(q_ref, qbuf.at[3], qs.at[1], qr.at[1], yl)),
    ]
    kv = [send_kv(0)]
    own = pltpu.make_async_copy(guo, gug.at[sp], loc)
    own.start()
    g = [send_g(0)]
    hy = [
        go(remote(guo.at[last], gug.at[sp, last], hs.at[i - 1], hr.at[i - 1], device(0, i)))
        for i in (1, 3, 2)
    ]
    ya = {0: send_ya(0)}
    yb = {}
    h = []

    top[...] = jnp.full(top.shape, -1e30, F32)
    total[...] = jnp.zeros(total.shape, F32)
    acc[...] = jnp.zeros(acc.shape, F32)
    row = lax.broadcasted_iota(jnp.int32, (2 * HD, 128), 0)

    def lay_queries(src, slot):
        for j in range(length // 128):
            turned = src[j * 128 : (j + 1) * 128, :].astype(F32).T * (LOG2E * HD**-0.5)
            for m in range(2):
                at = slot * cols + j * 256 + m * 128
                kept = jnp.where((row < HD) if m == 0 else (row >= HD), turned, 0.0)
                high = kept.astype(BF16)
                qbd[0:128, at : at + 128] = high
                qbd[128:256, at : at + 128] = (kept - high.astype(F32)).astype(BF16)

    def stage(slots):
        for n, s in enumerate(slots):
            kb = kslot(s)[...]
            kk[n * length : (n + 1) * length, 0:128] = kb
            kk[n * length : (n + 1) * length, 128:256] = kb
            vv[n * length : (n + 1) * length, :] = vslot(s)[...]

    def attend(count, begin, end):
        keys = count * length

        def tile(i, carry):
            at = pl.ds(pl.multiple_of(i * cols, cols), cols)
            scores = jnp.dot(kk[0:keys, :], qbd[:, at], preferred_element_type=F32)
            before = top[0:1, at]
            now = jnp.maximum(before, jnp.max(scores, axis=0, keepdims=True))
            shifted = jnp.exp2(scores - now)
            factor = jnp.exp2(before - now)
            top[0:1, at] = now
            total[0:1, at] = total[0:1, at] * factor + jnp.sum(shifted, axis=0, keepdims=True)
            acc[:, at] = acc[:, at] * factor + lax.dot_general(
                vv[0:keys, :],
                shifted.astype(BF16),
                (((0,), (0,)), ((), ())),
                preferred_element_type=F32,
            )
            return carry

        lax.fori_loop(begin, end, tile, 0)

    lay_queries(q_ref, 0)
    stage([0])
    attend(1, 0, 1)
    arrive(qa)
    low, high_rows = pl.ds(0, half), pl.ds(half, half)
    qb = [
        go(remote(qbuf.at[1, low], qbuf.at[2, low], qs.at[2], qr.at[2], yr)),
        go(remote(qbuf.at[3, high_rows], qbuf.at[2, high_rows], qs.at[3], qr.at[3], yl)),
    ]
    lay_queries(qbuf.at[1], 1)
    lay_queries(qbuf.at[3], 3)
    attend(1, 1, 2)
    attend(1, 3, 4)
    arrive(qb)
    lay_queries(qbuf.at[2], 2)
    attend(1, 2, 3)

    for t in range(1, 5):
        arrive(kv[t - 1])
        if t < 4:
            kv.append(send_kv(t))
        arrive(g[t - 1])
        if t < 4:
            g.append(send_g(t))
        if t == 2:
            arrive(hy)
            own.wait()
            h.append(send_h(0))
        elif t > 2:
            arrive(h[t - 3])
            h.append(send_h(t - 2))
        slots = [t, 8 - t] if t < 4 else [4]
        for s in slots:
            ya[s] = send_ya(s)
        for s in (0,) if t == 1 else (t - 1, 9 - t):
            arrive(ya[s])
            yb[s] = send_yb(s)
        stage(slots)
        attend(len(slots), 0, 4)

    for slot in range(4):
        for n in range(2):
            at = slice(slot * cols + n * length, slot * cols + (n + 1) * length)
            lse[0, 2 * slot + n : 2 * slot + n + 1, :] = top[0:1, at] + jnp.log2(total[0:1, at])
    stats = [
        go(remote(lse.at[0], lse.at[4 - i], ls.at[i - 1], lr.at[3 - i], device(0, i))) for i in (2, 1, 3)
    ]
    arrive(h[2])
    h.append(send_h(3))
    arrive(ya[4])
    yb[4] = send_yb(4)
    arrive(stats)
    weights = {}
    for slot in range(4):
        for n in range(2):
            logs = []
            for e in range(4):
                r = 2 * ((slot + e) % 4) + n
                logs.append(lse[e, r : r + 1, :])
            highest = jnp.maximum(jnp.maximum(logs[0], logs[1]), jnp.maximum(logs[2], logs[3]))
            shares = [jnp.exp2(v - highest) for v in logs]
            at = slice(slot * cols + n * length, slot * cols + (n + 1) * length)
            weights[slot, n] = shares[0] / ((shares[0] + shares[1] + shares[2] + shares[3]) * total[0:1, at])

    def mixture(slot, rows):
        out = []
        for j in range(length // 128):
            maps = []
            for m in range(2):
                at = j * 256 + m * 128
                w = weights[slot, at // length][:, at % length : at % length + 128]
                maps.append(acc[rows, slot * cols + at : slot * cols + at + 128] * w)
            out.append(maps[0] - lam_ref[0] * maps[1])
        return jnp.concatenate(out, axis=1)

    up_rows, low_rows = slice(0, 64), slice(64, 128)
    at_up, at_low = pl.ds(0, 64), pl.ds(64, 64)
    part[2, up_rows, :] = mixture(2, up_rows).astype(BF16)
    part[2, low_rows, :] = mixture(2, low_rows).astype(BF16)
    over = [
        go(remote(part.at[2, at_up], relay.at[0], ms.at[0], mr.at[0], yr)),
        go(remote(part.at[2, at_low], relay.at[1], ms.at[1], mr.at[1], yl)),
    ]
    part[3, low_rows, :] = mixture(3, low_rows).astype(BF16)
    part[1, up_rows, :] = mixture(1, up_rows).astype(BF16)
    ends = [
        go(remote(part.at[3, at_low], landed.at[0, at_low], ms.at[2], mr.at[2], yr)),
        go(remote(part.at[1, at_up], landed.at[1, at_up], ms.at[3], mr.at[3], yl)),
    ]
    third, firsts = mixture(3, up_rows), mixture(1, low_rows)
    arrive(over)
    part[3, up_rows, :] = (third + relay[0].astype(F32)).astype(BF16)
    part[1, low_rows, :] = (firsts + relay[1].astype(F32)).astype(BF16)
    ends += [
        go(remote(part.at[3, at_up], landed.at[0, at_up], ms.at[4], mr.at[4], yr)),
        go(remote(part.at[1, at_low], landed.at[1, at_low], ms.at[5], mr.at[5], yl)),
    ]
    mixed = mixture(0, slice(0, 128))
    arrive(ends)
    mixed = mixed + (landed[0].astype(F32) + landed[1].astype(F32))
    spread = jnp.mean(mixed * mixed, axis=0, keepdims=True)
    normed = mixed * lax.rsqrt(spread + 1e-06)
    gain = gain_ref[...][None, :] * 0.8
    for j in range(length // 128):
        at = slice(j * 128, (j + 1) * 128)
        out_ref[at, :] = (normed[:, at].T * gain).astype(BF16)

    for s in range(8):
        arrive(yb[s])
    arrive(h[3])
    for copy in started:
        copy.wait_send()


def attention(q, k, v, gate, up, lam, gain):
    length = q.shape[0]
    cols = 2 * length
    dma = pltpu.SemaphoreType.DMA
    rows, units = gate.shape
    return pl.pallas_call(
        attention_kernel,
        name="attention",
        out_shape=(
            jax.ShapeDtypeStruct((length, VD), BF16),
            jax.ShapeDtypeStruct((NZ * NY, rows, 2 * units), BF16),
        ),
        in_specs=[VMEM] * 5 + [SMEM, VMEM],
        out_specs=(VMEM, ANY),
        scratch_shapes=[
            pltpu.VMEM((rows, 2 * units), BF16),
            pltpu.VMEM((8, length, 128), BF16),
            pltpu.VMEM((8, length, 128), BF16),
            pltpu.VMEM((4, length, 128), BF16),
            pltpu.VMEM((2 * length, 256), BF16),
            pltpu.VMEM((2 * length, 128), BF16),
            pltpu.VMEM((256, 4 * cols), BF16),
            pltpu.VMEM((8, 4 * cols), F32),
            pltpu.VMEM((8, 4 * cols), F32),
            pltpu.VMEM((VD, 4 * cols), F32),
            pltpu.VMEM((4, 8, length), F32),
            pltpu.VMEM((4, VD, length), BF16),
            pltpu.VMEM((2, VD // 2, length), BF16),
            pltpu.VMEM((2, VD, length), BF16),
            dma((2, 4)),
            dma((8,)),
            dma((2, 4)),
            dma((8,)),
            dma((4,)),
            dma((4,)),
            dma((2, 4)),
            dma((2, 4)),
            dma((2, 8)),
            dma((2, 8)),
            dma((2, 8)),
            dma((2, 8)),
            dma((3,)),
            dma((3,)),
            dma((2, 4)),
            dma((2, 4)),
            dma((3,)),
            dma((3,)),
            dma((6,)),
            dma((6,)),
            dma,
        ],
        compiler_params=pltpu.CompilerParams(
            collective_id=0, has_side_effects=True, vmem_limit_bytes=60 * 2**20
        ),
    )(q, k, v, gate, up, lam, gain)


def tail_kernel(
    heads_ref,
    resid_ref,
    ow_ref,
    ng_ref,
    cw_ref,
    cb_ref,
    dw_ref,
    gug,
    out_ref,
    hall,
    nall,
    am,
    ssq,
    gu,
    big,
    gpad,
    gedge,
    halo,
    hid,
    dall,
    psib,
    rsib,
    pout,
    relayed,
    rout,
    keep,
    xs,
    xr,
    cs,
    cr,
    ts,
    tr,
    es,
    er,
    ys,
    yrr,
    zs,
    zrr,
    as_,
    ar,
    ya_s,
    ya_r,
    yb_s,
    yb_r,
    bs,
    br,
    ps,
    pr,
    loc,
):
    sp, tp = lax.axis_index("sp"), lax.axis_index("tp")
    z, y = sp // NY, sp % NY
    x, c = tp // 2, tp % 2
    length = heads_ref.shape[0]
    half = length // 2
    width = resid_ref.shape[1]
    units = dw_ref.shape[1]
    units_rows = dw_ref.shape[0]

    def xdev(dx, other=0):
        return (sp, ((x + dx) % 4) * 2 + (c + other) % 2)

    def index(dz, dy):
        return ((z + dz) % NZ) * NY + (y + dy) % NY

    def device(dz, dy):
        return (index(dz, dy), tp)

    xr_, xl_, sib = xdev(1), xdev(3), xdev(0, 1)
    zr, zl = device(1, 0), device(7, 0)
    yr, yl = device(0, 1), device(0, 3)
    hall[tp] = heads_ref[...]
    dall[sp] = dw_ref[...]
    after, before = ((sp + 1) % (NZ * NY), tp), ((sp + NZ * NY - 1) % (NZ * NY), tp)
    tp_peers = [(sp, (tp + i) % 8) for i in range(1, 8)]
    meet(tp_peers + [after, before, zr, zl] + [device(0, i) for i in (1, 2, 3)])
    started = []

    def go(copy):
        copy.start()
        started.append(copy)
        return copy

    def arrive(copies):
        for copy in copies:
            copy.wait_recv()

    load = pltpu.make_async_copy(gug, gu, loc)
    load.start()
    turn = units_rows // 2
    early, late = pl.ds(0, turn), pl.ds(turn, turn)
    upper_q, lower_q = pl.ds(0, turn // 2), pl.ds(turn // 2, turn // 2)

    def source(s, rows):
        return dw_ref.at[rows] if s == 0 else dall.at[index(8 - s, 0), rows]

    def send_a(t):
        right, left = t, (8 - t) % 8
        rows_r, rows_l = (upper_q, lower_q) if t == 3 else (early, early)
        return [
            go(remote(source(right, rows_r), dall.at[index(8 - right, 0), rows_r], as_.at[0, t], ar.at[0, t], zr)),
            go(remote(source(left, rows_l), dall.at[index(8 - left, 0), rows_l], as_.at[1, t], ar.at[1, t], zl)),
        ]

    def send_ya(s):
        dst = dall.at[index(8 - s, 0), early]
        return [
            go(remote(source(s, early), dst, ya_s.at[0, s], ya_r.at[0, s], yr)),
            go(remote(source(s, early), dst, ya_s.at[1, s], ya_r.at[1, s], yl)),
        ]

    def send_yb(s):
        a = dall.at[index(8 - s, 3), upper_q]
        b = dall.at[index(8 - s, 1), lower_q]
        return [
            go(remote(a, a, yb_s.at[0, s], yb_r.at[0, s], yr)),
            go(remote(b, b, yb_s.at[1, s], yb_r.at[1, s], yl)),
        ]

    def send_d(t):
        right, left = ((z + 8 - t) % NZ) * NY, ((z + t) % NZ) * NY
        if t < 3:
            a, b = dall.at[pl.ds(right, NY), late], dall.at[pl.ds(left, NY), late]
        else:
            a, b = dall.at[pl.ds(right, 2), late], dall.at[pl.ds(left + 2, 2), late]
        return [
            go(remote(a, a, zs.at[0, t], zrr.at[0, t], zr)),
            go(remote(b, b, zs.at[1, t], zrr.at[1, t], zl)),
        ]

    def gather(stack, k):
        mine = stack.at[tp]
        one = [
            go(remote(mine, mine, xs.at[k, 0], xr.at[k, 0], xr_)),
            go(remote(mine, mine, xs.at[k, 1], xr.at[k, 1], xl_)),
        ]
        core = [go(remote(mine, mine, cs.at[k, 0], cr.at[k, 0], sib))]
        yield None
        arrive(core)
        yield 0
        from_left = stack.at[((x + 3) % 4) * 2 + c]
        from_right = stack.at[((x + 1) % 4) * 2 + c]
        upper, lower = pl.ds(0, half), pl.ds(half, half)
        arrive(one[:1])
        two = [go(remote(from_left.at[upper], from_left.at[upper], xs.at[k, 2], xr.at[k, 2], xr_))]
        core.append(go(remote(from_left, from_left, cs.at[k, 1], cr.at[k, 1], sib)))
        arrive(one[1:])
        two.append(go(remote(from_right.at[lower], from_right.at[lower], xs.at[k, 3], xr.at[k, 3], xl_)))
        core.append(go(remote(from_right, from_right, cs.at[k, 2], cr.at[k, 2], sib)))
        arrive(core[1:2])
        yield 3
        arrive(core[2:3])
        yield 1
        far = stack.at[((x + 2) % 4) * 2 + c]
        arrive(two[:1])
        core.append(go(remote(far.at[upper], far.at[upper], cs.at[k, 3], cr.at[k, 3], sib)))
        arrive(two[1:])
        core.append(go(remote(far.at[lower], far.at[lower], cs.at[k, 4], cr.at[k, 4], sib)))
        arrive(core[3:5])
        yield 2

    heads = gather(hall, 0)
    next(heads)
    da = [send_a(0)]
    along = [
        go(remote(dw_ref.at[late], dall.at[sp, late], ys.at[i - 1], yrr.at[i - 1], device(0, i)))
        for i in (1, 3, 2)
    ]
    ya, yb, dz = {0: send_ya(0)}, {}, []
    am[...] = resid_ref[...].astype(F32)

    def relay_a(t):
        arrive(da[t])
        if t < 3:
            da.append(send_a(t + 1))
        for s in (t + 1, 7 - t) if t < 3 else (4,):
            ya[s] = send_ya(s)

    def relay_y(*slots):
        for s in slots:
            arrive(ya[s])
            yb[s] = send_yb(s)

    def relay_d(t):
        arrive(along if t == 0 else dz[t - 1])
        dz.append(send_d(t))

    for n, dx in enumerate(heads):
        chip = (x + dx) % 4
        for core in range(2):
            rows = pl.ds(pl.multiple_of((chip * 2 + core) * VD, VD), VD)
            am[...] += jnp.dot(hall[chip * 2 + core], ow_ref[rows, :], preferred_element_type=F32)
        if n == 0:
            relay_a(0)
            relay_d(0)
            relay_y(0)
        elif n == 2:
            relay_a(1)
            relay_y(1, 7)
    value = am[...]
    nall[tp] = (value * ng_ref[...][None, :]).astype(BF16)
    rows_in = gather(nall, 1)
    next(rows_in)
    square = value * value
    square = square[:, 0:128] + square[:, 128:256]
    for j in range(length // 128):
        ssq[tp, j : j + 1, :] = jnp.sum(square[j * 128 : (j + 1) * 128, :].T, axis=0, keepdims=True)
    ssq[tp, length // 128 :, :] = jnp.zeros((8 - length // 128, 128), F32)
    tiny = [
        go(remote(ssq.at[tp], ssq.at[tp], ts.at[i - 1], tr.at[i - 1], (sp, (tp + i) % 8)))
        for i in range(1, 8)
    ]
    relay_a(2)
    relay_y(2, 6)
    relay_d(1)
    load.wait()

    def product(chip):
        a = jnp.concatenate([nall[chip * 2], nall[chip * 2 + 1]], axis=1)
        rows = pl.ds(pl.multiple_of(chip * 2 * width, 2 * width), 2 * width)
        return jnp.dot(a, gu[rows, :], preferred_element_type=F32)

    for n, dx in enumerate(rows_in):
        if n == 0:
            big[...] = product((x + dx) % 4)
            relay_a(3)
            relay_y(3, 5)
        else:
            big[...] += product((x + dx) % 4)
        if n == 2:
            relay_d(2)
            relay_y(4)
    relay_d(3)
    arrive(tiny)
    squares = ssq[0]
    for i in range(1, 8):
        squares = squares + ssq[i]
    factor = lax.rsqrt(squares * (1.0 / D) + 1e-06)
    whole = units // 128 * 128
    rest = units - whole
    for j in range(length // 128):
        rows = slice(j * 128, (j + 1) * 128)
        column = jnp.broadcast_to(factor[j : j + 1, :], (128, 128)).T[:, 0:1]
        scaled = big[rows, :] * column
        gate = jnp.concatenate([scaled[:, 0:whole], scaled[:, 2 * whole : 2 * whole + rest]], axis=1)
        gpad[8 + j * 128 : 8 + (j + 1) * 128, :] = gate.astype(BF16).astype(F32)
        big[rows, whole:] = scaled[:, whole:]
    gedge[0] = gpad[8:24, :].astype(BF16)
    gedge[1] = gpad[8 + length - 16 : 8 + length, :].astype(BF16)
    edge = [
        go(remote(gedge.at[1], halo.at[0], es.at[0], er.at[0], after)),
        go(remote(gedge.at[0], halo.at[1], es.at[1], er.at[1], before)),
    ]
    arrive(edge)
    previous = jnp.where(sp == 0, 0.0, halo[0].astype(F32)[15:16, :])
    following = jnp.where(sp == NZ * NY - 1, 0.0, halo[1].astype(F32)[0:1, :])
    gpad[7:8, :] = previous
    gpad[8 + length : 9 + length, :] = following
    for j in range(length // 128):
        rows = slice(j * 128, (j + 1) * 128)
        at = 8 + j * 128
        conv = (
            gpad[at - 1 : at + 127, :] * cw_ref[0:1, :]
            + gpad[at : at + 128, :] * cw_ref[1:2, :]
            + gpad[at + 1 : at + 129, :] * cw_ref[2:3, :]
            + cb_ref[...][None, :]
        )
        up = jnp.concatenate([big[rows, whole : 2 * whole], big[rows, 2 * whole + rest :]], axis=1)
        hid[rows, :] = (conv / (1.0 + jnp.exp(-conv)) * up).astype(BF16)

    for s in range(8):
        arrive(yb[s])
    arrive(dz[3])
    per = width // units_rows

    def down(target):
        w = dall[pl.ds(target * per, per)].reshape(width, units)
        return lax.dot_general(
            hid[...], w, (((1,), (1,)), ((), ())), preferred_element_type=F32
        )

    order = (2, 1, 3, 0)
    crossing = {}
    for dx in order:
        psib[dx] = down(((x + dx) % 4) * 2 + (1 - c)).astype(BF16)
        crossing[dx] = go(remote(psib.at[dx], rsib.at[dx], bs.at[dx], br.at[dx], sib))
    upper, lower = slice(0, half), slice(half, length)
    at_upper, at_lower = pl.ds(0, half), pl.ds(half, half)
    ends = []
    for dx in order:
        piece = down(((x + dx) % 4) * 2 + c)
        arrive([crossing[dx]])
        piece = piece + rsib[dx].astype(F32)
        if dx == 2:
            pout[2] = piece.astype(BF16)
            over = [
                go(remote(pout.at[2, at_upper], relayed.at[0], ps.at[0], pr.at[0], xr_)),
                go(remote(pout.at[2, at_lower], relayed.at[1], ps.at[1], pr.at[1], xl_)),
            ]
        elif dx == 1:
            pout[1, lower, :] = piece[lower, :].astype(BF16)
            ends.append(go(remote(pout.at[1, at_lower], rout.at[0, at_lower], ps.at[2], pr.at[2], xr_)))
            keep[0] = piece[upper, :]
        elif dx == 3:
            pout[3, upper, :] = piece[upper, :].astype(BF16)
            ends.append(go(remote(pout.at[3, at_upper], rout.at[1, at_upper], ps.at[3], pr.at[3], xl_)))
            keep[1] = piece[lower, :]
            arrive(over)
            pout[1, upper, :] = (keep[0] + relayed[0].astype(F32)).astype(BF16)
            ends.append(go(remote(pout.at[1, at_upper], rout.at[0, at_upper], ps.at[4], pr.at[4], xr_)))
            pout[3, lower, :] = (keep[1] + relayed[1].astype(F32)).astype(BF16)
            ends.append(go(remote(pout.at[3, at_lower], rout.at[1, at_lower], ps.at[5], pr.at[5], xl_)))
        else:
            am[...] += piece
    arrive(ends)
    out_ref[...] = (am[...] + (rout[0].astype(F32) + rout[1].astype(F32))).astype(BF16)
    for copy in started:
        copy.wait_send()


def tail(heads, resid, ow, ng, cw, cb, dw, gug):
    length, width = resid.shape
    units = dw.shape[1]
    dma = pltpu.SemaphoreType.DMA
    return pl.pallas_call(
        tail_kernel,
        name="tail",
        out_shape=jax.ShapeDtypeStruct((length, width), BF16),
        in_specs=[VMEM] * 7 + [ANY],
        out_specs=VMEM,
        scratch_shapes=[
            pltpu.VMEM((8, length, VD), BF16),
            pltpu.VMEM((8, length, width), BF16),
            pltpu.VMEM((length, width), F32),
            pltpu.VMEM((8, 8, 128), F32),
            pltpu.VMEM(gug.shape, BF16),
            pltpu.VMEM((length, 2 * units), F32),
            pltpu.VMEM((length + 16, units), F32),
            pltpu.VMEM((2, 16, units), BF16),
            pltpu.VMEM((2, 16, units), BF16),
            pltpu.VMEM((length, units), BF16),
            pltpu.VMEM((NZ * NY, *dw.shape), BF16),
            pltpu.VMEM((4, length, width), BF16),
            pltpu.VMEM((4, length, width), BF16),
            pltpu.VMEM((4, length, width), BF16),
            pltpu.VMEM((2, length // 2, width), BF16),
            pltpu.VMEM((2, length, width), BF16),
            pltpu.VMEM((2, length // 2, width), F32),
            dma((2, 4)),
            dma((2, 4)),
            dma((2, 5)),
            dma((2, 5)),
            dma((7,)),
            dma((7,)),
            dma((2,)),
            dma((2,)),
            dma((3,)),
            dma((3,)),
            dma((2, 4)),
            dma((2, 4)),
            dma((2, 4)),
            dma((2, 4)),
            dma((2, 8)),
            dma((2, 8)),
            dma((2, 8)),
            dma((2, 8)),
            dma((4,)),
            dma((4,)),
            dma((6,)),
            dma((6,)),
            dma,
        ],
        compiler_params=pltpu.CompilerParams(
            collective_id=1, has_side_effects=True, vmem_limit_bytes=60 * 2**20
        ),
    )(heads, resid, ow, ng, cw, cb, dw, gug)


def on_device(
    resid,
    queries,
    keys,
    values,
    mix_lambda,
    head_gain,
    out_weight,
    norm_gain,
    gate_weight,
    up_weight,
    conv_weight,
    conv_bias,
    down_weight,
):
    heads_out, gug = attention(queries, keys, values, gate_weight, up_weight, mix_lambda, head_gain)
    return tail(
        heads_out,
        resid,
        out_weight,
        norm_gain,
        conv_weight,
        conv_bias,
        down_weight.T,
        gug.reshape(-1, gug.shape[-1]),
    )


def solution(mesh):
    return jax.shard_map(
        on_device,
        mesh=mesh,
        in_specs=(
            P("sp", "tp"),
            P("sp", "tp"),
            P("sp", "tp"),
            P("sp", "tp"),
            P("tp"),
            P(),
            P(None, "tp"),
            P("tp"),
            P("sp", "tp"),
            P("sp", "tp"),
            P(None, "tp"),
            P("tp"),
            P("tp", "sp"),
        ),
        out_specs=P("sp", "tp"),
        check_vma=False,
    )
```

time: 162 us -> 131 us (0.81)
  Pallas kernels: 153 us -> 128 us
  local copies, waits for them, and re-layouts: 8.77 us -> 1.67 us
    pallas_call x1, Pallas kernels: 74 us -> 59.6 us  [tail(): pl.pallas_call(tail_kernel, name='tail', out_shape=jax.ShapeDtypeStruct((...]
    pallas_call x1, Pallas kernels: 78.7 us -> 68.5 us  [attention(): pl.pallas_call(attention_kernel, name='attention', out_shape=(jax.ShapeDt...]
    slice x4 -> x0, local copies, waits for them, and re-layouts: 3.22 us -> none  [the longest x1 0.89 us: on_device(): up_weight[:, :whole]]
    broadcast_in_dim x3 -> x0, local copies, waits for them, and re-layouts: 3.12 us -> none  [the longest x1 1.28 us: on_device(): conv_bias[None, :]]
where the time goes in v2:
time: 131 us; the launch traced here: 130 us
  Pallas kernels  128 us (98%)
  local copies, waits for them, and re-layouts  1.67 us (1%)
    pallas_call x1, Pallas kernels, attention(): pl.pallas_call(attention_kernel, name='attention', out_shape=(jax.ShapeDt...  68.5 us
    pallas_call x1, Pallas kernels, tail(): pl.pallas_call(tail_kernel, name='tail', out_shape=jax.ShapeDtypeStruct((...  59.6 us

profile of v2, /device:TPU:1, one launch (start us, length us, event | category | flops | bytes accessed | tf_op | source)
XLA Modules:
  0.0 130.5 jit_solution(16280532904300800957)
XLA Ops:
  0.7 68.5 %attention.1 = (bf16[512,128]{1,0:T(8,128)(2,1)}, bf16[32,64,1408]{2,1,0:T(8,128)(2,1)}) custom-call(bf16[512,128]{1,0:T(8,128)(2,1)} %q_ref.1, bf16[512,128]{1,0:T(8,128)(2,1)} %k_ref.1, bf16[512,128]{1,0:T(8,128)(2,1)} %v_ref.1, bf16[64,704]{1,0:T(8,128)(2,1)} %gate_ref.1, bf16[64,704]{1,0:T(8,128)(2,1)} %up_ref.1, f32[1]{0:T(128)S(6)} %copy.15.lam_ref, ...), custom_call_target="tpu_custom_call" | custom-call | tf_op jit(solution)/shard_map/attention/pallas_call | solution.py:352
  69.2 59.6 %tail.1 = bf16[512,256]{1,0:T(8,128)(2,1)} custom-call(bf16[512,128]{1,0:T(8,128)(2,1)} %get-tuple-element.7.heads_ref, bf16[512,256]{1,0:T(8,128)(2,1)} %resid_ref.1, bf16[1024,256]{1,0:T(8,128)(2,1)} %ow_ref.1, f32[256]{0:T(256)} %ng_ref.1, f32[3,704]{1,0:T(4,128)} %cw_ref.1, f32[704]{0:T(1024)} %cb_ref.1, bf16[64,704]{1,0:T(8,128)(2,1)} %bitcast.3, ...), custom_call_target="tpu_custom_call" | custom-call | tf_op jit(solution)/shard_map/tail/pallas_call | solution.py:729
  128.8 1.7 %copy.16 = bf16[512,256]{1,0:T(8,128)(2,1)} copy(bf16[512,256]{1,0:T(8,128)(2,1)} %tail.1) | data formatting | bytes 524288

commit v3 on v2

v3 whole, which is shorter than its diff:
```python
import jax
import jax.numpy as jnp
from jax import lax
from jax.experimental import pallas as pl
from jax.experimental.pallas import tpu as pltpu
from jax.sharding import PartitionSpec as P

D = 2048
HD = 64
VD = 128
LOG2E = 1.4426950408889634
NZ = 8
NY = 4
F32 = jnp.float32
BF16 = jnp.bfloat16
MESH = pl.DeviceIdType.MESH
VMEM = pl.BlockSpec(memory_space=pltpu.VMEM)
ANY = pl.BlockSpec(memory_space=pl.ANY)
SMEM = pl.BlockSpec(memory_space=pltpu.SMEM)


def remote(src, dst, send, recv, device):
    return pltpu.make_async_remote_copy(
        src_ref=src, dst_ref=dst, send_sem=send, recv_sem=recv, device_id=device, device_id_type=MESH
    )


def meet(peers):
    barrier = pltpu.get_barrier_semaphore()
    for peer in peers:
        pl.semaphore_signal(barrier, inc=1, device_id=peer, device_id_type=MESH)
    pl.semaphore_wait(barrier, len(peers))


def layer_kernel(
    q_ref,
    k_ref,
    v_ref,
    gate_ref,
    up_ref,
    lam_ref,
    gain_ref,
    resid_ref,
    ow_ref,
    ng_ref,
    cw_ref,
    cb_ref,
    dw_ref,
    out_ref,
    *,
    gug,
    kbuf,
    vbuf,
    qbuf,
    kk,
    vv,
    qbd,
    top,
    total,
    acc,
    lse,
    part,
    relay,
    landed,
    hall,
    nall,
    am,
    ssq,
    big,
    gpad,
    gedge,
    halo,
    hid,
    dall,
    psib,
    rsib,
    pout,
    relayed,
    rout,
    keep,
    ks,
    kr,
    vs,
    vr,
    qs,
    qr,
    gs,
    gr,
    ya_s,
    ya_r,
    yb_s,
    yb_r,
    hs,
    hr,
    hz_s,
    hz_r,
    ls,
    lr,
    ms,
    mr,
    xs,
    xr,
    cs,
    cr,
    ts,
    tr,
    es,
    er,
    ys,
    yrr,
    zs,
    zrr,
    as_,
    ar,
    dya_s,
    dya_r,
    dyb_s,
    dyb_r,
    bs,
    br,
    ps,
    pr,
):
    sp, tp = lax.axis_index("sp"), lax.axis_index("tp")
    z, y = sp // NY, sp % NY
    length = q_ref.shape[0]
    cols = 2 * length
    half = length // 2
    units = gate_ref.shape[1]
    whole = units // 128 * 128
    rest = units - whole
    first = pl.ds(0, 48)
    last = pl.ds(48, 16)

    def index(dz, dy):
        return ((z + dz) % NZ) * NY + (y + dy) % NY

    def device(dz, dy):
        return (index(dz, dy), tp)

    zr, zl = device(1, 0), device(7, 0)
    yr, yl = device(0, 1), device(0, 3)
    gug[sp, :, 0:whole] = gate_ref[:, 0:whole]
    gug[sp, :, whole : 2 * whole] = up_ref[:, 0:whole]
    gug[sp, :, 2 * whole :] = jnp.concatenate([gate_ref[:, whole:], up_ref[:, whole:]], axis=1)
    dall[sp] = dw_ref[...]
    am[...] = resid_ref[...].astype(F32)
    x, c = tp // 2, tp % 2
    width = resid_ref.shape[1]
    units_rows = dw_ref.shape[0]

    def xdev(dx, other=0):
        return (sp, ((x + dx) % 4) * 2 + (c + other) % 2)

    xr_, xl_, sib = xdev(1), xdev(3), xdev(0, 1)
    after, before_ = ((sp + 1) % (NZ * NY), tp), ((sp + NZ * NY - 1) % (NZ * NY), tp)
    tp_peers = [(sp, (tp + i) % 8) for i in range(1, 8)]
    meet([zr, zl, yr, yl, device(0, 2)] + tp_peers + [after, before_])
    started = []

    def go(copy):
        copy.start()
        started.append(copy)
        return copy

    def arrive(copies):
        for copy in copies:
            copy.wait_recv()

    def kslot(s):
        return k_ref if s == 0 else kbuf.at[s]

    def vslot(s):
        return v_ref if s == 0 else vbuf.at[s]

    def send_kv(t):
        right, left = t, (8 - t) % 8
        out = [go(remote(kslot(right), kbuf.at[t + 1], ks.at[0, t], kr.at[t + 1], zr))]
        if t < 3:
            out.append(go(remote(kslot(left), kbuf.at[7 - t], ks.at[1, t], kr.at[7 - t], zl)))
            out.append(go(remote(vslot(right), vbuf.at[t + 1], vs.at[0, t], vr.at[t + 1], zr)))
        out.append(go(remote(vslot(left), vbuf.at[7 - t], vs.at[1, t], vr.at[7 - t], zl)))
        return out

    def source(s, rows):
        return gug.at[index(8 - s, 0), rows]

    def parts(s):
        return (pl.ds(0, 16), pl.ds(16, 32)) if s % 2 == 0 else (pl.ds(0, 32), pl.ds(32, 16))

    def send_g(t):
        right, left = t, (8 - t) % 8
        rows_r, rows_l = parts(0) if t == 3 else (first, first)
        return [
            go(remote(source(right, rows_r), gug.at[index(8 - right, 0), rows_r], gs.at[0, t], gr.at[0, t], zr)),
            go(remote(source(left, rows_l), gug.at[index(8 - left, 0), rows_l], gs.at[1, t], gr.at[1, t], zl)),
        ]

    def send_ya(s):
        dst = gug.at[index(8 - s, 0), first]
        return [
            go(remote(source(s, first), dst, ya_s.at[0, s], ya_r.at[0, s], yr)),
            go(remote(source(s, first), dst, ya_s.at[1, s], ya_r.at[1, s], yl)),
        ]

    def send_yb(s):
        rows_r, rows_l = parts(s)
        a = gug.at[index(8 - s, 3), rows_r]
        b = gug.at[index(8 - s, 1), rows_l]
        return [
            go(remote(a, a, yb_s.at[0, s], yb_r.at[0, s], yr)),
            go(remote(b, b, yb_s.at[1, s], yb_r.at[1, s], yl)),
        ]

    def send_h(t):
        right, left = ((z + 8 - t) % NZ) * NY, ((z + t) % NZ) * NY
        if t < 3:
            a, b = gug.at[pl.ds(right, NY), last], gug.at[pl.ds(left, NY), last]
        else:
            a, b = gug.at[pl.ds(right, 2), last], gug.at[pl.ds(left + 2, 2), last]
        return [
            go(remote(a, a, hz_s.at[0, t], hz_r.at[0, t], zr)),
            go(remote(b, b, hz_s.at[1, t], hz_r.at[1, t], zl)),
        ]

    da, dya, dyb, dz = [], {}, {}, []
    turn = units_rows // 2
    early, late = pl.ds(0, turn), pl.ds(turn, turn)
    upper_q, lower_q = pl.ds(0, turn // 2), pl.ds(turn // 2, turn // 2)

    def dsource(s, rows):
        return dall.at[index(8 - s, 0), rows]

    def send_a(t):
        right, left = t, (8 - t) % 8
        rows_r, rows_l = (upper_q, lower_q) if t == 3 else (early, early)
        return [
            go(remote(dsource(right, rows_r), dall.at[index(8 - right, 0), rows_r], as_.at[0, t], ar.at[0, t], zr)),
            go(remote(dsource(left, rows_l), dall.at[index(8 - left, 0), rows_l], as_.at[1, t], ar.at[1, t], zl)),
        ]

    def send_dya(s):
        dst = dall.at[index(8 - s, 0), early]
        return [
            go(remote(dsource(s, early), dst, dya_s.at[0, s], dya_r.at[0, s], yr)),
            go(remote(dsource(s, early), dst, dya_s.at[1, s], dya_r.at[1, s], yl)),
        ]

    def send_dyb(s):
        a = dall.at[index(8 - s, 3), upper_q]
        b = dall.at[index(8 - s, 1), lower_q]
        return [
            go(remote(a, a, dyb_s.at[0, s], dyb_r.at[0, s], yr)),
            go(remote(b, b, dyb_s.at[1, s], dyb_r.at[1, s], yl)),
        ]

    def send_d(t):
        right, left = ((z + 8 - t) % NZ) * NY, ((z + t) % NZ) * NY
        if t < 3:
            a, b = dall.at[pl.ds(right, NY), late], dall.at[pl.ds(left, NY), late]
        else:
            a, b = dall.at[pl.ds(right, 2), late], dall.at[pl.ds(left + 2, 2), late]
        return [
            go(remote(a, a, zs.at[0, t], zrr.at[0, t], zr)),
            go(remote(b, b, zs.at[1, t], zrr.at[1, t], zl)),
        ]

    def gather(stack, k):
        mine = stack.at[tp]
        one = [
            go(remote(mine, mine, xs.at[k, 0], xr.at[k, 0], xr_)),
            go(remote(mine, mine, xs.at[k, 1], xr.at[k, 1], xl_)),
        ]
        core = [go(remote(mine, mine, cs.at[k, 0], cr.at[k, 0], sib))]
        yield None
        arrive(core)
        yield 0
        from_left = stack.at[((x + 3) % 4) * 2 + c]
        from_right = stack.at[((x + 1) % 4) * 2 + c]
        upper, lower = pl.ds(0, half), pl.ds(half, half)
        arrive(one[:1])
        two = [go(remote(from_left.at[upper], from_left.at[upper], xs.at[k, 2], xr.at[k, 2], xr_))]
        core.append(go(remote(from_left, from_left, cs.at[k, 1], cr.at[k, 1], sib)))
        arrive(one[1:])
        two.append(go(remote(from_right.at[lower], from_right.at[lower], xs.at[k, 3], xr.at[k, 3], xl_)))
        core.append(go(remote(from_right, from_right, cs.at[k, 2], cr.at[k, 2], sib)))
        arrive(core[1:2])
        yield 3
        arrive(core[2:3])
        yield 1
        far = stack.at[((x + 2) % 4) * 2 + c]
        arrive(two[:1])
        core.append(go(remote(far.at[upper], far.at[upper], cs.at[k, 3], cr.at[k, 3], sib)))
        arrive(two[1:])
        core.append(go(remote(far.at[lower], far.at[lower], cs.at[k, 4], cr.at[k, 4], sib)))
        arrive(core[3:5])
        yield 2

    def relay_a(t):
        arrive(da[t])
        if t < 3:
            da.append(send_a(t + 1))
        for s in (t + 1, 7 - t) if t < 3 else (4,):
            dya[s] = send_dya(s)

    def relay_y(*slots):
        for s in slots:
            arrive(dya[s])
            dyb[s] = send_dyb(s)

    def relay_d(t, along=None):
        arrive(along if t == 0 else dz[t - 1])
        dz.append(send_d(t))

    qa = [
        go(remote(q_ref, qbuf.at[1], qs.at[0], qr.at[0], yr)),
        go(remote(q_ref, qbuf.at[3], qs.at[1], qr.at[1], yl)),
    ]
    kv = [send_kv(0)]
    g = [send_g(0)]
    hy = [
        go(remote(gug.at[sp, last], gug.at[sp, last], hs.at[i - 1], hr.at[i - 1], device(0, i)))
        for i in (1, 3, 2)
    ]
    ya = {0: send_ya(0)}
    yb = {}
    h = []

    top[...] = jnp.full(top.shape, -1e30, F32)
    total[...] = jnp.zeros(total.shape, F32)
    acc[...] = jnp.zeros(acc.shape, F32)
    row = lax.broadcasted_iota(jnp.int32, (2 * HD, 128), 0)

    def lay_queries(src, slot):
        for j in range(length // 128):
            turned = src[j * 128 : (j + 1) * 128, :].astype(F32).T * (LOG2E * HD**-0.5)
            for m in range(2):
                at = slot * cols + j * 256 + m * 128
                kept = jnp.where((row < HD) if m == 0 else (row >= HD), turned, 0.0)
                high = kept.astype(BF16)
                qbd[0:128, at : at + 128] = high
                qbd[128:256, at : at + 128] = (kept - high.astype(F32)).astype(BF16)

    def stage(slots):
        for n, s in enumerate(slots):
            kb = kslot(s)[...]
            kk[n * length : (n + 1) * length, 0:128] = kb
            kk[n * length : (n + 1) * length, 128:256] = kb
            vv[n * length : (n + 1) * length, :] = vslot(s)[...]

    def attend(count, begin, end):
        keys = count * length

        def tile(i, carry):
            at = pl.ds(pl.multiple_of(i * cols, cols), cols)
            scores = jnp.dot(kk[0:keys, :], qbd[:, at], preferred_element_type=F32)
            before = top[0:1, at]
            now = jnp.maximum(before, jnp.max(scores, axis=0, keepdims=True))
            shifted = jnp.exp2(scores - now)
            factor = jnp.exp2(before - now)
            top[0:1, at] = now
            total[0:1, at] = total[0:1, at] * factor + jnp.sum(shifted, axis=0, keepdims=True)
            acc[:, at] = acc[:, at] * factor + lax.dot_general(
                vv[0:keys, :],
                shifted.astype(BF16),
                (((0,), (0,)), ((), ())),
                preferred_element_type=F32,
            )
            return carry

        lax.fori_loop(begin, end, tile, 0)

    lay_queries(q_ref, 0)
    stage([0])
    attend(1, 0, 1)
    arrive(qa)
    low, high_rows = pl.ds(0, half), pl.ds(half, half)
    qb = [
        go(remote(qbuf.at[1, low], qbuf.at[2, low], qs.at[2], qr.at[2], yr)),
        go(remote(qbuf.at[3, high_rows], qbuf.at[2, high_rows], qs.at[3], qr.at[3], yl)),
    ]
    lay_queries(qbuf.at[1], 1)
    lay_queries(qbuf.at[3], 3)
    attend(1, 1, 2)
    attend(1, 3, 4)
    arrive(qb)
    lay_queries(qbuf.at[2], 2)
    attend(1, 2, 3)

    for t in range(1, 5):
        arrive(kv[t - 1])
        if t < 4:
            kv.append(send_kv(t))
        slots = [t, 8 - t] if t < 4 else [4]
        stage(slots)
        attend(len(slots), 0, 2)
        arrive(g[t - 1])
        if t < 4:
            g.append(send_g(t))
            for s in slots:
                ya[s] = send_ya(s)
            for s in (0,) if t == 1 else (t - 1, 9 - t):
                arrive(ya[s])
                yb[s] = send_yb(s)
        else:
            arrive(hy)
            h.append(send_h(0))
        attend(len(slots), 2, 4)

    for slot in range(4):
        for n in range(2):
            at = slice(slot * cols + n * length, slot * cols + (n + 1) * length)
            lse[0, 2 * slot + n : 2 * slot + n + 1, :] = top[0:1, at] + jnp.log2(total[0:1, at])
    stats = [
        go(remote(lse.at[0], lse.at[4 - i], ls.at[i - 1], lr.at[3 - i], device(0, i))) for i in (2, 1, 3)
    ]
    arrive(stats)
    weights = {}
    for slot in range(4):
        for n in range(2):
            logs = []
            for e in range(4):
                r = 2 * ((slot + e) % 4) + n
                logs.append(lse[e, r : r + 1, :])
            highest = jnp.maximum(jnp.maximum(logs[0], logs[1]), jnp.maximum(logs[2], logs[3]))
            shares = [jnp.exp2(v - highest) for v in logs]
            at = slice(slot * cols + n * length, slot * cols + (n + 1) * length)
            weights[slot, n] = shares[0] / ((shares[0] + shares[1] + shares[2] + shares[3]) * total[0:1, at])

    def mixture(slot, rows):
        out = []
        for j in range(length // 128):
            maps = []
            for m in range(2):
                at = j * 256 + m * 128
                w = weights[slot, at // length][:, at % length : at % length + 128]
                maps.append(acc[rows, slot * cols + at : slot * cols + at + 128] * w)
            out.append(maps[0] - lam_ref[0] * maps[1])
        return jnp.concatenate(out, axis=1)

    up_rows, low_rows = slice(0, 64), slice(64, 128)
    at_up, at_low = pl.ds(0, 64), pl.ds(64, 64)
    part[2, up_rows, :] = mixture(2, up_rows).astype(BF16)
    part[2, low_rows, :] = mixture(2, low_rows).astype(BF16)
    over = [
        go(remote(part.at[2, at_up], relay.at[0], ms.at[0], mr.at[0], yr)),
        go(remote(part.at[2, at_low], relay.at[1], ms.at[1], mr.at[1], yl)),
    ]
    part[3, low_rows, :] = mixture(3, low_rows).astype(BF16)
    part[1, up_rows, :] = mixture(1, up_rows).astype(BF16)
    ends = [
        go(remote(part.at[3, at_low], landed.at[0, at_low], ms.at[2], mr.at[2], yr)),
        go(remote(part.at[1, at_up], landed.at[1, at_up], ms.at[3], mr.at[3], yl)),
    ]
    third, firsts = mixture(3, up_rows), mixture(1, low_rows)
    arrive(h[0])
    h.append(send_h(1))
    arrive(over)
    part[3, up_rows, :] = (third + relay[0].astype(F32)).astype(BF16)
    part[1, low_rows, :] = (firsts + relay[1].astype(F32)).astype(BF16)
    ends += [
        go(remote(part.at[3, at_up], landed.at[0, at_up], ms.at[4], mr.at[4], yr)),
        go(remote(part.at[1, at_low], landed.at[1, at_low], ms.at[5], mr.at[5], yl)),
    ]
    ya[4] = send_ya(4)
    for s in (3, 5):
        arrive(ya[s])
        yb[s] = send_yb(s)
    da.append(send_a(0))
    dya[0] = send_dya(0)
    mixed = mixture(0, slice(0, 128))
    arrive(ends)
    mixed = mixed + (landed[0].astype(F32) + landed[1].astype(F32))
    spread = jnp.mean(mixed * mixed, axis=0, keepdims=True)
    normed = mixed * lax.rsqrt(spread + 1e-06)
    gain = gain_ref[...][None, :] * 0.8
    for j in range(length // 128):
        at = slice(j * 128, (j + 1) * 128)
        hall[tp, at, :] = (normed[:, at].T * gain).astype(BF16)
    heads = gather(hall, 0)
    next(heads)
    along = [
        go(remote(dall.at[sp, late], dall.at[sp, late], ys.at[i - 1], yrr.at[i - 1], device(0, i)))
        for i in (1, 3, 2)
    ]
    arrive(h[1])
    h.append(send_h(2))
    arrive(ya[4])
    yb[4] = send_yb(4)
    for n, dx in enumerate(heads):
        chip = (x + dx) % 4
        for core in range(2):
            rows = pl.ds(pl.multiple_of((chip * 2 + core) * VD, VD), VD)
            am[...] += jnp.dot(hall[chip * 2 + core], ow_ref[rows, :], preferred_element_type=F32)
        if n == 0:
            relay_a(0)
            relay_d(0, along)
        elif n == 2:
            arrive(h[2])
            h.append(send_h(3))
            relay_a(1)
            relay_y(0)
    value = am[...]
    nall[tp] = (value * ng_ref[...][None, :]).astype(BF16)
    rows_in = gather(nall, 1)
    next(rows_in)
    square = value * value
    square = square[:, 0:128] + square[:, 128:256]
    for j in range(length // 128):
        ssq[tp, j : j + 1, :] = jnp.sum(square[j * 128 : (j + 1) * 128, :].T, axis=0, keepdims=True)
    ssq[tp, length // 128 :, :] = jnp.zeros((8 - length // 128, 128), F32)
    tiny = [
        go(remote(ssq.at[tp], ssq.at[tp], ts.at[i - 1], tr.at[i - 1], (sp, (tp + i) % 8)))
        for i in range(1, 8)
    ]
    relay_a(2)
    relay_y(1, 7)
    relay_d(1)
    for s in range(8):
        arrive(yb[s])
    arrive(h[3])

    def product(chip):
        a = jnp.concatenate([nall[chip * 2], nall[chip * 2 + 1]], axis=1)
        per_chip = 2 * width // units_rows
        return jnp.dot(a, gug[pl.ds(chip * per_chip, per_chip)].reshape(2 * width, 2 * units), preferred_element_type=F32)

    for n, dx in enumerate(rows_in):
        if n == 0:
            big[...] = product((x + dx) % 4)
            relay_a(3)
            relay_y(2, 6)
        else:
            big[...] += product((x + dx) % 4)
        if n == 2:
            relay_d(2)
            relay_y(3, 5)
    relay_d(3)
    relay_y(4)
    arrive(tiny)
    squares = ssq[0]
    for i in range(1, 8):
        squares = squares + ssq[i]
    factor = lax.rsqrt(squares * (1.0 / D) + 1e-06)
    for j in range(length // 128):
        rows = slice(j * 128, (j + 1) * 128)
        column = jnp.broadcast_to(factor[j : j + 1, :], (128, 128)).T[:, 0:1]
        scaled = big[rows, :] * column
        gate = jnp.concatenate([scaled[:, 0:whole], scaled[:, 2 * whole : 2 * whole + rest]], axis=1)
        gpad[8 + j * 128 : 8 + (j + 1) * 128, :] = gate.astype(BF16).astype(F32)
        big[rows, whole:] = scaled[:, whole:]
    gedge[0] = gpad[8:24, :].astype(BF16)
    gedge[1] = gpad[8 + length - 16 : 8 + length, :].astype(BF16)
    edge = [
        go(remote(gedge.at[1], halo.at[0], es.at[0], er.at[0], after)),
        go(remote(gedge.at[0], halo.at[1], es.at[1], er.at[1], before_)),
    ]

    def convolve(j):
        rows = slice(j * 128, (j + 1) * 128)
        at = 8 + j * 128
        conv = (
            gpad[at - 1 : at + 127, :] * cw_ref[0:1, :]
            + gpad[at : at + 128, :] * cw_ref[1:2, :]
            + gpad[at + 1 : at + 129, :] * cw_ref[2:3, :]
            + cb_ref[...][None, :]
        )
        up = jnp.concatenate([big[rows, whole : 2 * whole], big[rows, 2 * whole + rest :]], axis=1)
        hid[rows, :] = (conv / (1.0 + jnp.exp(-conv)) * up).astype(BF16)

    for j in range(1, length // 128 - 1):
        convolve(j)
    arrive(edge)
    gpad[7:8, :] = jnp.where(sp == 0, 0.0, halo[0].astype(F32)[15:16, :])
    gpad[8 + length : 9 + length, :] = jnp.where(sp == NZ * NY - 1, 0.0, halo[1].astype(F32)[0:1, :])
    convolve(0)
    convolve(length // 128 - 1)

    for s in range(8):
        arrive(dyb[s])
    arrive(dz[3])
    per = width // units_rows

    def down(target):
        w = dall[pl.ds(target * per, per)].reshape(width, units)
        return lax.dot_general(
            hid[...], w, (((1,), (1,)), ((), ())), preferred_element_type=F32
        )

    order = (2, 1, 3, 0)
    crossing = {}
    for dx in order:
        psib[dx] = down(((x + dx) % 4) * 2 + (1 - c)).astype(BF16)
        crossing[dx] = go(remote(psib.at[dx], rsib.at[dx], bs.at[dx], br.at[dx], sib))
    upper, lower = slice(0, half), slice(half, length)
    at_upper, at_lower = pl.ds(0, half), pl.ds(half, half)
    ends = []
    for dx in order:
        piece = down(((x + dx) % 4) * 2 + c)
        arrive([crossing[dx]])
        piece = piece + rsib[dx].astype(F32)
        if dx == 2:
            pout[2] = piece.astype(BF16)
            over = [
                go(remote(pout.at[2, at_upper], relayed.at[0], ps.at[0], pr.at[0], xr_)),
                go(remote(pout.at[2, at_lower], relayed.at[1], ps.at[1], pr.at[1], xl_)),
            ]
        elif dx == 1:
            pout[1, lower, :] = piece[lower, :].astype(BF16)
            ends.append(go(remote(pout.at[1, at_lower], rout.at[0, at_lower], ps.at[2], pr.at[2], xr_)))
            keep[0] = piece[upper, :]
        elif dx == 3:
            pout[3, upper, :] = piece[upper, :].astype(BF16)
            ends.append(go(remote(pout.at[3, at_upper], rout.at[1, at_upper], ps.at[3], pr.at[3], xl_)))
            keep[1] = piece[lower, :]
            arrive(over)
            pout[1, upper, :] = (keep[0] + relayed[0].astype(F32)).astype(BF16)
            ends.append(go(remote(pout.at[1, at_upper], rout.at[0, at_upper], ps.at[4], pr.at[4], xr_)))
            pout[3, lower, :] = (keep[1] + relayed[1].astype(F32)).astype(BF16)
            ends.append(go(remote(pout.at[3, at_lower], rout.at[1, at_lower], ps.at[5], pr.at[5], xl_)))
        else:
            am[...] += piece
    arrive(ends)
    out_ref[...] = (am[...] + (rout[0].astype(F32) + rout[1].astype(F32))).astype(BF16)
    for copy in started:
        copy.wait_send()


def layer(q, k, v, gate, up, lam, gain, resid, ow, ng, cw, cb, dw):
    length, width = resid.shape
    cols = 2 * length
    rows, units = gate.shape
    half = length // 2
    dma, vmem = pltpu.SemaphoreType.DMA, pltpu.VMEM
    scratch = dict(
        gug=vmem((NZ * NY, rows, 2 * units), BF16),
        kbuf=vmem((8, length, 128), BF16),
        vbuf=vmem((8, length, 128), BF16),
        qbuf=vmem((4, length, 128), BF16),
        kk=vmem((2 * length, 256), BF16),
        vv=vmem((2 * length, 128), BF16),
        qbd=vmem((256, 4 * cols), BF16),
        top=vmem((8, 4 * cols), F32),
        total=vmem((8, 4 * cols), F32),
        acc=vmem((VD, 4 * cols), F32),
        lse=vmem((4, 8, length), F32),
        part=vmem((4, VD, length), BF16),
        relay=vmem((2, VD // 2, length), BF16),
        landed=vmem((2, VD, length), BF16),
        hall=vmem((8, length, VD), BF16),
        nall=vmem((8, length, width), BF16),
        am=vmem((length, width), F32),
        ssq=vmem((8, 8, 128), F32),
        big=vmem((length, 2 * units), F32),
        gpad=vmem((length + 16, units), F32),
        gedge=vmem((2, 16, units), BF16),
        halo=vmem((2, 16, units), BF16),
        hid=vmem((length, units), BF16),
        dall=vmem((NZ * NY, *dw.shape), BF16),
        psib=vmem((4, length, width), BF16),
        rsib=vmem((4, length, width), BF16),
        pout=vmem((4, length, width), BF16),
        relayed=vmem((2, half, width), BF16),
        rout=vmem((2, length, width), BF16),
        keep=vmem((2, half, width), F32),
    )
    semaphores = dict(
        ks=(2, 4), kr=(8,), vs=(2, 4), vr=(8,), qs=(4,), qr=(4,), gs=(2, 4), gr=(2, 4),
        ya_s=(2, 8), ya_r=(2, 8), yb_s=(2, 8), yb_r=(2, 8), hs=(3,), hr=(3,), hz_s=(2, 4), hz_r=(2, 4),
        ls=(3,), lr=(3,), ms=(6,), mr=(6,), xs=(2, 4), xr=(2, 4), cs=(2, 5), cr=(2, 5), ts=(7,), tr=(7,),
        es=(2,), er=(2,), ys=(3,), yrr=(3,), zs=(2, 4), zrr=(2, 4), as_=(2, 4), ar=(2, 4),
        dya_s=(2, 8), dya_r=(2, 8), dyb_s=(2, 8), dyb_r=(2, 8), bs=(4,), br=(4,), ps=(6,), pr=(6,),
    )
    return pl.pallas_call(
        layer_kernel,
        name="layer",
        out_shape=jax.ShapeDtypeStruct((length, width), BF16),
        in_specs=[VMEM] * 5 + [SMEM] + [VMEM] * 7,
        out_specs=VMEM,
        scratch_shapes=dict(scratch, **{n: dma(shape) for n, shape in semaphores.items()}),
        compiler_params=pltpu.CompilerParams(
            collective_id=0, has_side_effects=True, vmem_limit_bytes=63 * 2**20
        ),
    )(q, k, v, gate, up, lam, gain, resid, ow, ng, cw, cb, dw)


def on_device(
    resid,
    queries,
    keys,
    values,
    mix_lambda,
    head_gain,
    out_weight,
    norm_gain,
    gate_weight,
    up_weight,
    conv_weight,
    conv_bias,
    down_weight,
):
    return layer(
        queries,
        keys,
        values,
        gate_weight,
        up_weight,
        mix_lambda,
        head_gain,
        resid,
        out_weight,
        norm_gain,
        conv_weight,
        conv_bias,
        down_weight.T,
    )


def solution(mesh):
    return jax.shard_map(
        on_device,
        mesh=mesh,
        in_specs=(
            P("sp", "tp"),
            P("sp", "tp"),
            P("sp", "tp"),
            P("sp", "tp"),
            P("tp"),
            P(),
            P(None, "tp"),
            P("tp"),
            P("sp", "tp"),
            P("sp", "tp"),
            P(None, "tp"),
            P("tp"),
            P("tp", "sp"),
        ),
        out_specs=P("sp", "tp"),
        check_vma=False,
    )
```

time: 131 us -> 121 us (0.924)
  Pallas kernels: 128 us -> 118 us
    pallas_call x2 -> x1, Pallas kernels: 128 us -> 118 us  [layer(): pl.pallas_call(layer_kernel, name='layer', out_shape=jax.ShapeDtypeStruct...]
where the time goes in v3:
time: 121 us
  Pallas kernels  118 us (98%)
  local copies, waits for them, and re-layouts  1.67 us (1%)
    pallas_call x1, Pallas kernels, layer(): pl.pallas_call(layer_kernel, name='layer', out_shape=jax.ShapeDtypeStruct...  118 us

profile of v3, /device:TPU:1, one launch (start us, length us, event | category | flops | bytes accessed | tf_op | source)
XLA Modules:
  0.0 120.5 jit_solution(9016467889777009072)
XLA Ops:
  0.7 118.2 %layer.1 = bf16[512,256]{1,0:T(8,128)(2,1)} custom-call(bf16[512,128]{1,0:T(8,128)(2,1)} %q_ref.1, bf16[512,128]{1,0:T(8,128)(2,1)} %k_ref.1, bf16[512,128]{1,0:T(8,128)(2,1)} %v_ref.1, bf16[64,704]{1,0:T(8,128)(2,1)} %gate_ref.1, bf16[64,704]{1,0:T(8,128)(2,1)} %up_ref.1, f32[1]{0:T(128)S(6)} %copy.15.lam_ref, f32[128]{0:T(128)} %gain_ref.1, ...), custom_call_target="tpu_custom_call" | custom-call | tf_op jit(solution)/shard_map/layer/pallas_call | solution.py:674
  118.9 1.7 %copy.16 = bf16[512,256]{1,0:T(8,128)(2,1)} copy(bf16[512,256]{1,0:T(8,128)(2,1)} %layer.1) | data formatting | bytes 524288

commit v4 on v3

--- a/solution.py
+++ b/solution.py
@@ -265,8 +265,12 @@
             go(remote(b, b, zs.at[1, t], zrr.at[1, t], zl)),
         ]
 
-    def gather(stack, k):
-        mine = stack.at[tp]
+    quarter = half // 2
+
+    def gather(stack, k, begin):
+        here = pl.ds(begin, half)
+        upper, lower = pl.ds(begin, quarter), pl.ds(begin + quarter, quarter)
+        mine = stack.at[tp, here]
         one = [
             go(remote(mine, mine, xs.at[k, 0], xr.at[k, 0], xr_)),
             go(remote(mine, mine, xs.at[k, 1], xr.at[k, 1], xl_)),
@@ -275,24 +279,23 @@
         yield None
         arrive(core)
         yield 0
-        from_left = stack.at[((x + 3) % 4) * 2 + c]
-        from_right = stack.at[((x + 1) % 4) * 2 + c]
-        upper, lower = pl.ds(0, half), pl.ds(half, half)
+        left, right = ((x + 3) % 4) * 2 + c, ((x + 1) % 4) * 2 + c
         arrive(one[:1])
-        two = [go(remote(from_left.at[upper], from_left.at[upper], xs.at[k, 2], xr.at[k, 2], xr_))]
-        core.append(go(remote(from_left, from_left, cs.at[k, 1], cr.at[k, 1], sib)))
+        two = [go(remote(stack.at[left, upper], stack.at[left, upper], xs.at[k, 2], xr.at[k, 2], xr_))]
+        core.append(go(remote(stack.at[left, here], stack.at[left, here], cs.at[k, 1], cr.at[k, 1], sib)))
         arrive(one[1:])
-        two.append(go(remote(from_right.at[lower], from_right.at[lower], xs.at[k, 3], xr.at[k, 3], xl_)))
-        core.append(go(remote(from_right, from_right, cs.at[k, 2], cr.at[k, 2], sib)))
+        two.append(go(remote(stack.at[right, lower], stack.at[right, lower], xs.at[k, 3], xr.at[k, 3], xl_)))
+        core.append(go(remote(stack.at[right, here], stack.at[right, here], cs.at[k, 2], cr.at[k, 2], sib)))
+        yield None
         arrive(core[1:2])
         yield 3
         arrive(core[2:3])
         yield 1
-        far = stack.at[((x + 2) % 4) * 2 + c]
+        far = ((x + 2) % 4) * 2 + c
         arrive(two[:1])
-        core.append(go(remote(far.at[upper], far.at[upper], cs.at[k, 3], cr.at[k, 3], sib)))
+        core.append(go(remote(stack.at[far, upper], stack.at[far, upper], cs.at[k, 3], cr.at[k, 3], sib)))
         arrive(two[1:])
-        core.append(go(remote(far.at[lower], far.at[lower], cs.at[k, 4], cr.at[k, 4], sib)))
+        core.append(go(remote(stack.at[far, lower], stack.at[far, lower], cs.at[k, 4], cr.at[k, 4], sib)))
         arrive(core[3:5])
         yield 2
 
@@ -352,20 +355,21 @@
         keys = count * length
 
         def tile(i, carry):
-            at = pl.ds(pl.multiple_of(i * cols, cols), cols)
-            scores = jnp.dot(kk[0:keys, :], qbd[:, at], preferred_element_type=F32)
-            before = top[0:1, at]
-            now = jnp.maximum(before, jnp.max(scores, axis=0, keepdims=True))
-            shifted = jnp.exp2(scores - now)
-            factor = jnp.exp2(before - now)
-            top[0:1, at] = now
-            total[0:1, at] = total[0:1, at] * factor + jnp.sum(shifted, axis=0, keepdims=True)
-            acc[:, at] = acc[:, at] * factor + lax.dot_general(
-                vv[0:keys, :],
-                shifted.astype(BF16),
-                (((0,), (0,)), ((), ())),
-                preferred_element_type=F32,
-            )
+            halves = [pl.ds(pl.multiple_of(i * cols + n * length, length), length) for n in range(2)]
+            scores = [jnp.dot(kk[0:keys, :], qbd[:, at], preferred_element_type=F32) for at in halves]
+            for at, score in zip(halves, scores):
+                before = top[0:1, at]
+                now = jnp.maximum(before, jnp.max(score, axis=0, keepdims=True))
+                shifted = jnp.exp2(score - now)
+                factor = jnp.exp2(before - now)
+                top[0:1, at] = now
+                total[0:1, at] = total[0:1, at] * factor + jnp.sum(shifted, axis=0, keepdims=True)
+                acc[:, at] = acc[:, at] * factor + lax.dot_general(
+                    vv[0:keys, :],
+                    shifted.astype(BF16),
+                    (((0,), (0,)), ((), ())),
+                    preferred_element_type=F32,
+                )
             return carry
 
         lax.fori_loop(begin, end, tile, 0)
@@ -402,9 +406,14 @@
             for s in (0,) if t == 1 else (t - 1, 9 - t):
                 arrive(ya[s])
                 yb[s] = send_yb(s)
+            if t == 3:
+                arrive(hy)
+                h.append(send_h(0))
         else:
-            arrive(hy)
-            h.append(send_h(0))
+            along = [
+                go(remote(dall.at[sp, late], dall.at[sp, late], ys.at[i - 1], yrr.at[i - 1], device(0, i)))
+                for i in (1, 3, 2)
+            ]
         attend(len(slots), 2, 4)
 
     for slot in range(4):
@@ -414,6 +423,9 @@
     stats = [
         go(remote(lse.at[0], lse.at[4 - i], ls.at[i - 1], lr.at[3 - i], device(0, i))) for i in (2, 1, 3)
     ]
+    arrive(h[0])
+    h.append(send_h(1))
+    da.append(send_a(0))
     arrive(stats)
     weights = {}
     for slot in range(4):
@@ -453,8 +465,6 @@
         go(remote(part.at[1, at_up], landed.at[1, at_up], ms.at[3], mr.at[3], yl)),
     ]
     third, firsts = mixture(3, up_rows), mixture(1, low_rows)
-    arrive(h[0])
-    h.append(send_h(1))
     arrive(over)
     part[3, up_rows, :] = (third + relay[0].astype(F32)).astype(BF16)
     part[1, low_rows, :] = (firsts + relay[1].astype(F32)).astype(BF16)
@@ -466,44 +476,56 @@
     for s in (3, 5):
         arrive(ya[s])
         yb[s] = send_yb(s)
-    da.append(send_a(0))
     dya[0] = send_dya(0)
+    arrive(h[1])
+    h.append(send_h(2))
+    relay_a(0)
+    relay_d(0, along)
     mixed = mixture(0, slice(0, 128))
     arrive(ends)
     mixed = mixed + (landed[0].astype(F32) + landed[1].astype(F32))
     spread = jnp.mean(mixed * mixed, axis=0, keepdims=True)
     normed = mixed * lax.rsqrt(spread + 1e-06)
     gain = gain_ref[...][None, :] * 0.8
+    parts_of = [slice(n * half, (n + 1) * half) for n in range(2)]
+    heads, rows_in = [], []
     for j in range(length // 128):
         at = slice(j * 128, (j + 1) * 128)
         hall[tp, at, :] = (normed[:, at].T * gain).astype(BF16)
-    heads = gather(hall, 0)
-    next(heads)
-    along = [
-        go(remote(dall.at[sp, late], dall.at[sp, late], ys.at[i - 1], yrr.at[i - 1], device(0, i)))
-        for i in (1, 3, 2)
-    ]
-    arrive(h[1])
-    h.append(send_h(2))
+        if (j + 1) * 128 % half == 0:
+            n = len(heads)
+            heads.append(gather(hall, n, n * half))
+            next(heads[n])
+
+    def project(dx, n):
+        chip = (x + dx) % 4
+        for core in range(2):
+            w = pl.ds(pl.multiple_of((chip * 2 + core) * VD, VD), VD)
+            am[parts_of[n], :] += jnp.dot(
+                hall[chip * 2 + core, parts_of[n], :], ow_ref[w, :], preferred_element_type=F32
+            )
+
+    for n in range(2):
+        project(next(heads[n]), n)
+    arrive(h[2])
+    h.append(send_h(3))
     arrive(ya[4])
     yb[4] = send_yb(4)
-    for n, dx in enumerate(heads):
-        chip = (x + dx) % 4
-        for core in range(2):
-            rows = pl.ds(pl.multiple_of((chip * 2 + core) * VD, VD), VD)
-            am[...] += jnp.dot(hall[chip * 2 + core], ow_ref[rows, :], preferred_element_type=F32)
-        if n == 0:
-            relay_a(0)
-            relay_d(0, along)
-        elif n == 2:
-            arrive(h[2])
-            h.append(send_h(3))
-            relay_a(1)
-            relay_y(0)
+    relay_y(0)
+    for n in range(2):
+        next(heads[n])
+    for step in range(2):
+        for n in range(2):
+            project(next(heads[n]), n)
+    relay_a(1)
+    relay_y(1, 7)
+    relay_d(1)
+    for n in range(2):
+        project(next(heads[n]), n)
+        nall[tp, parts_of[n], :] = (am[parts_of[n], :] * ng_ref[...][None, :]).astype(BF16)
+        rows_in.append(gather(nall, 2 + n, n * half))
+        next(rows_in[n])
     value = am[...]
-    nall[tp] = (value * ng_ref[...][None, :]).astype(BF16)
-    rows_in = gather(nall, 1)
-    next(rows_in)
     square = value * value
     square = square[:, 0:128] + square[:, 128:256]
     for j in range(length // 128):
@@ -513,30 +535,33 @@
         go(remote(ssq.at[tp], ssq.at[tp], ts.at[i - 1], tr.at[i - 1], (sp, (tp + i) % 8)))
         for i in range(1, 8)
     ]
-    relay_a(2)
-    relay_y(1, 7)
-    relay_d(1)
     for s in range(8):
         arrive(yb[s])
     arrive(h[3])
 
-    def product(chip):
-        a = jnp.concatenate([nall[chip * 2], nall[chip * 2 + 1]], axis=1)
-        per_chip = 2 * width // units_rows
-        return jnp.dot(a, gug[pl.ds(chip * per_chip, per_chip)].reshape(2 * width, 2 * units), preferred_element_type=F32)
-
-    for n, dx in enumerate(rows_in):
-        if n == 0:
-            big[...] = product((x + dx) % 4)
-            relay_a(3)
-            relay_y(2, 6)
-        else:
-            big[...] += product((x + dx) % 4)
-        if n == 2:
-            relay_d(2)
-            relay_y(3, 5)
+    per_chip = 2 * width // units_rows
+
+    def product(dx, n):
+        chip = (x + dx) % 4
+        a = jnp.concatenate([nall[chip * 2, parts_of[n], :], nall[chip * 2 + 1, parts_of[n], :]], axis=1)
+        w = gug[pl.ds(chip * per_chip, per_chip)].reshape(2 * width, 2 * units)
+        return jnp.dot(a, w, preferred_element_type=F32)
+
+    for n in range(2):
+        big[parts_of[n], :] = product(next(rows_in[n]), n)
+    for n in range(2):
+        next(rows_in[n])
+    relay_a(2)
+    relay_d(2)
+    relay_y(2, 6)
+    for step in range(2):
+        for n in range(2):
+            big[parts_of[n], :] += product(next(rows_in[n]), n)
+    for n in range(2):
+        big[parts_of[n], :] += product(next(rows_in[n]), n)
+    relay_a(3)
+    relay_y(3, 5)
     relay_d(3)
-    relay_y(4)
     arrive(tiny)
     squares = ssq[0]
     for i in range(1, 8):
@@ -570,6 +595,7 @@
 
     for j in range(1, length // 128 - 1):
         convolve(j)
+    relay_y(4)
     arrive(edge)
     gpad[7:8, :] = jnp.where(sp == 0, 0.0, halo[0].astype(F32)[15:16, :])
     gpad[8 + length : 9 + length, :] = jnp.where(sp == NZ * NY - 1, 0.0, halo[1].astype(F32)[0:1, :])
@@ -667,7 +693,7 @@
     semaphores = dict(
         ks=(2, 4), kr=(8,), vs=(2, 4), vr=(8,), qs=(4,), qr=(4,), gs=(2, 4), gr=(2, 4),
         ya_s=(2, 8), ya_r=(2, 8), yb_s=(2, 8), yb_r=(2, 8), hs=(3,), hr=(3,), hz_s=(2, 4), hz_r=(2, 4),
-        ls=(3,), lr=(3,), ms=(6,), mr=(6,), xs=(2, 4), xr=(2, 4), cs=(2, 5), cr=(2, 5), ts=(7,), tr=(7,),
+        ls=(3,), lr=(3,), ms=(6,), mr=(6,), xs=(4, 4), xr=(4, 4), cs=(4, 5), cr=(4, 5), ts=(7,), tr=(7,),
         es=(2,), er=(2,), ys=(3,), yrr=(3,), zs=(2, 4), zrr=(2, 4), as_=(2, 4), ar=(2, 4),
         dya_s=(2, 8), dya_r=(2, 8), dyb_s=(2, 8), dyb_r=(2, 8), bs=(4,), br=(4,), ps=(6,), pr=(6,),
     )

time: 121 us -> 118 us (0.975)
  Pallas kernels: 118 us -> 115 us
    pallas_call x1, Pallas kernels: 118 us -> 115 us  [layer(): pl.pallas_call(layer_kernel, name='layer', out_shape=jax.ShapeDtypeStruct...]
where the time goes in v4:
time: 118 us; the launch traced here: 117 us
  Pallas kernels  115 us (97%)
  local copies, waits for them, and re-layouts  1.67 us (1%)
    pallas_call x1, Pallas kernels, layer(): pl.pallas_call(layer_kernel, name='layer', out_shape=jax.ShapeDtypeStruct...  115 us

profile of v4, /device:TPU:1, one launch (start us, length us, event | category | flops | bytes accessed | tf_op | source)
XLA Modules:
  0.0 117.3 jit_solution(1359982540830316903)
XLA Ops:
  0.7 115.0 %layer.1 = bf16[512,256]{1,0:T(8,128)(2,1)} custom-call(bf16[512,128]{1,0:T(8,128)(2,1)} %q_ref.1, bf16[512,128]{1,0:T(8,128)(2,1)} %k_ref.1, bf16[512,128]{1,0:T(8,128)(2,1)} %v_ref.1, bf16[64,704]{1,0:T(8,128)(2,1)} %gate_ref.1, bf16[64,704]{1,0:T(8,128)(2,1)} %up_ref.1, f32[1]{0:T(128)S(6)} %copy.15.lam_ref, f32[128]{0:T(128)} %gain_ref.1, ...), custom_call_target="tpu_custom_call" | custom-call | tf_op jit(solution)/shard_map/layer/pallas_call | solution.py:700
  115.6 1.7 %copy.16 = bf16[512,256]{1,0:T(8,128)(2,1)} copy(bf16[512,256]{1,0:T(8,128)(2,1)} %layer.1) | data formatting | bytes 524288

commit v5 on v4

--- a/solution.py
+++ b/solution.py
@@ -507,13 +507,13 @@
 
     for n in range(2):
         project(next(heads[n]), n)
+    for n in range(2):
+        next(heads[n])
     arrive(h[2])
     h.append(send_h(3))
     arrive(ya[4])
     yb[4] = send_yb(4)
     relay_y(0)
-    for n in range(2):
-        next(heads[n])
     for step in range(2):
         for n in range(2):
             project(next(heads[n]), n)
@@ -535,9 +535,6 @@
         go(remote(ssq.at[tp], ssq.at[tp], ts.at[i - 1], tr.at[i - 1], (sp, (tp + i) % 8)))
         for i in range(1, 8)
     ]
-    for s in range(8):
-        arrive(yb[s])
-    arrive(h[3])
 
     per_chip = 2 * width // units_rows
 
@@ -548,12 +545,17 @@
         return jnp.dot(a, w, preferred_element_type=F32)
 
     for n in range(2):
-        big[parts_of[n], :] = product(next(rows_in[n]), n)
+        next(rows_in[n])
     for n in range(2):
         next(rows_in[n])
     relay_a(2)
     relay_d(2)
     relay_y(2, 6)
+    for s in range(8):
+        arrive(yb[s])
+    arrive(h[3])
+    for n in range(2):
+        big[parts_of[n], :] = product(0, n)
     for step in range(2):
         for n in range(2):
             big[parts_of[n], :] += product(next(rows_in[n]), n)

time: 118 us -> 116 us (0.983)
  no operation moved by 1% of the time
where the time goes in v5:
time: 116 us
  Pallas kernels  114 us (98%)
  local copies, waits for them, and re-layouts  1.67 us (1%)
    pallas_call x1, Pallas kernels, layer(): pl.pallas_call(layer_kernel, name='layer', out_shape=jax.ShapeDtypeStruct...  114 us

profile of v5, /device:TPU:1, one launch (start us, length us, event | category | flops | bytes accessed | tf_op | source)
XLA Modules:
  0.0 116.2 jit_solution(2170526988501734861)
XLA Ops:
  0.7 113.9 %layer.1 = bf16[512,256]{1,0:T(8,128)(2,1)} custom-call(bf16[512,128]{1,0:T(8,128)(2,1)} %q_ref.1, bf16[512,128]{1,0:T(8,128)(2,1)} %k_ref.1, bf16[512,128]{1,0:T(8,128)(2,1)} %v_ref.1, bf16[64,704]{1,0:T(8,128)(2,1)} %gate_ref.1, bf16[64,704]{1,0:T(8,128)(2,1)} %up_ref.1, f32[1]{0:T(128)S(6)} %copy.15.lam_ref, f32[128]{0:T(128)} %gain_ref.1, ...), custom_call_target="tpu_custom_call" | custom-call | tf_op jit(solution)/shard_map/layer/pallas_call | solution.py:702
  114.6 1.7 %copy.16 = bf16[512,256]{1,0:T(8,128)(2,1)} copy(bf16[512,256]{1,0:T(8,128)(2,1)} %layer.1) | data formatting | bytes 524288
